TPU v7x, 32 devices: a whole 2x2x4 slice. The times are simulated.
32 devices in a mesh: st: 8 (over z, y), tp: 4 (over x, core).
Axes of the slice: x: 2, y: 2, z: 4, core: 2. Of those that a mesh axis runs over, the one named last changes fastest.
Arguments:
- queries: bfloat16 [8192, 1024], P('st', 'tp'), may hold values from -540 to 540
- gate_pre: bfloat16 [8192, 1024], P('st', 'tp'), may hold values from -6 to 6
- cotangent: bfloat16 [8192, 1024], P('st', 'tp'), may hold values from -6 to 6
- store: bfloat16 [10240, 2048], P('st'), may hold values from -6 to 6
- store_gain: float32 [2048], replicated, may hold values from 0.1 to 1.9
- w_key: bfloat16 [2048, 1024], P(None, 'tp'), may hold values from -0.125 to 0.125
- w_value: bfloat16 [2048, 1024], P(None, 'tp'), may hold values from -0.125 to 0.125
- owners: int32 [64, 4], P('st'), may hold values from 0 to 7, all different within a row; in each aligned block of 8 rows (0 to 7, 8 to 15, ...) at most 8 rows name the same one
- slots: int32 [64, 4], P('st'), may hold values from 0 to 19
Outputs:
- grad_queries: float32 [8192, 1024], P('st', 'tp')
- grad_store: float32 [10240, 2048], P(('st', 'tp'))
- grad_w_value: float32 [2048, 1024], P('st', 'tp')
Inputs may be any that keep to these rules, and one draw needn't show every extreme that they name: Each block names 4 different owners. Among the blocks of one device no owner is named twice.
All inputs are finite; a program needn't handle non-finite values.
Results may differ from a plain program's by a relative error of at most 0.014.
Values may be sent and summed in bfloat16 or wider, within the bound.
A program may use at most 192 MiB of HBM per device.

v0:
```python
import functools

import jax
import jax.numpy as jnp
from jax import lax
from jax.experimental import pallas as pl
from jax.experimental.pallas import tpu as pltpu
from jax.sharding import PartitionSpec as P

HD = 128
PLEN = 64


EPS = 1e-06


def row_scale(store_rows):
    return lax.rsqrt(jnp.mean(store_rows * store_rows, axis=-1, keepdims=True) + EPS)


def contract(left, right):
    return lax.dot_general(
        left, right, (((1,), (1,)), ((), ())), preferred_element_type=jnp.float32
    )


def passage_plan(queries, gate_pre, cotangent, store, store_gain, w_key, w_value, owners, slots):
    st_size = lax.axis_size("st")
    tp_size = lax.axis_size("tp")
    blocks, per_block = owners.shape
    tok_rows, local_width = queries.shape
    head_dim = HD
    local_heads = local_width // head_dim
    block_len = tok_rows // blocks
    passage_len = PLEN
    rows_dev = store.shape[0]
    passages = rows_dev // passage_len
    slot_count = blocks * per_block
    slot_cap = (2 * slot_count + st_size - 1) // st_size
    store_rows = store.astype(jnp.float32)
    row_inverse = row_scale(store_rows)
    normed = (store_rows * row_inverse * store_gain).astype(jnp.bfloat16)
    key_table = jnp.dot(normed, w_key, preferred_element_type=jnp.float32).astype(jnp.bfloat16)
    value_table = jnp.dot(normed, w_value, preferred_element_type=jnp.float32).astype(jnp.bfloat16)
    key_table = key_table.reshape(passages, passage_len, local_width)
    value_table = value_table.reshape(passages, passage_len, local_width)
    owner_flat = owners.reshape(slot_count)
    slot_flat = slots.reshape(slot_count)
    slot_order = jnp.arange(slot_count, dtype=jnp.int32)
    earlier_same = (owner_flat[:, None] == owner_flat[None, :]) & (
        slot_order[None, :] < slot_order[:, None]
    )
    slot_rank = jnp.sum(earlier_same.astype(jnp.int32), axis=1)
    position = owner_flat * slot_cap + slot_rank
    places = jnp.arange(st_size * slot_cap, dtype=jnp.int32)
    slot_hits = position[:, None] == places[None, :]
    requests = jnp.sum(jnp.where(slot_hits, slot_flat[:, None], 0), axis=0)
    requests = requests.reshape(st_size, slot_cap)
    asked_ids = lax.all_to_all(requests, "st", split_axis=0, concat_axis=0, tiled=True)
    asked_flat = asked_ids.reshape(-1)
    shape_out = asked_ids.shape + (passage_len, local_width)
    picked_keys = jnp.take(key_table, asked_flat, axis=0).reshape(shape_out)
    picked_values = jnp.take(value_table, asked_flat, axis=0).reshape(shape_out)
    sent_keys = lax.all_to_all(picked_keys, "st", split_axis=0, concat_axis=0, tiled=True)
    sent_values = lax.all_to_all(picked_values, "st", split_axis=0, concat_axis=0, tiled=True)
    got_keys, got_values, asked_ids = (sent_keys, sent_values, asked_ids)
    span = per_block * passage_len
    mine_keys = jnp.take(
        got_keys.reshape(st_size * slot_cap, passage_len, local_width), position, axis=0
    )
    mine_values = jnp.take(
        got_values.reshape(st_size * slot_cap, passage_len, local_width), position, axis=0
    )
    mine_keys = mine_keys.reshape(blocks, span, local_heads, head_dim)
    mine_values = mine_values.reshape(blocks, span, local_heads, head_dim)
    score_scale = head_dim ** (-0.5)
    query_blocks = queries.reshape(blocks, block_len, local_heads, head_dim)
    gate_open = jax.nn.sigmoid(gate_pre.astype(jnp.float32))
    grad_in = (gate_open * cotangent.astype(jnp.float32)).astype(jnp.bfloat16)
    grad_in = grad_in.reshape(blocks, block_len, local_heads, head_dim)
    scores = (
        jnp.einsum("bqhd,bkhd->bhqk", query_blocks, mine_keys, preferred_element_type=jnp.float32)
        * score_scale
    )
    shifted = scores - jnp.max(scores, axis=-1, keepdims=True)
    weights = jnp.exp(shifted)
    weights = weights / jnp.sum(weights, axis=-1, keepdims=True)
    weights_half = weights.astype(jnp.bfloat16)
    attended = jnp.einsum(
        "bhqk,bkhd->bqhd", weights_half, mine_values, preferred_element_type=jnp.float32
    )
    row_delta = jnp.sum(grad_in.astype(jnp.float32) * attended, axis=-1)
    grad_weights = jnp.einsum(
        "bqhd,bkhd->bhqk", grad_in, mine_values, preferred_element_type=jnp.float32
    )
    grad_scores = weights * (grad_weights - jnp.transpose(row_delta, (0, 2, 1))[..., None])
    grad_half = grad_scores.astype(jnp.bfloat16)
    grad_queries = (
        jnp.einsum("bhqk,bkhd->bqhd", grad_half, mine_keys, preferred_element_type=jnp.float32)
        * score_scale
    )
    grad_queries = grad_queries.reshape(tok_rows, local_width)
    grad_keys = (
        jnp.einsum("bhqk,bqhd->bkhd", grad_half, query_blocks, preferred_element_type=jnp.float32)
        * score_scale
    )
    grad_values = jnp.einsum(
        "bhqk,bqhd->bkhd", weights_half, grad_in, preferred_element_type=jnp.float32
    )
    grad_keys = grad_keys.reshape(slot_count, passage_len, local_width)
    grad_values = grad_values.reshape(slot_count, passage_len, local_width)
    empty_slots = jnp.zeros((st_size * slot_cap, passage_len, local_width), jnp.bfloat16)
    outgoing_keys = empty_slots.at[position].set(grad_keys.astype(jnp.bfloat16))
    outgoing_values = empty_slots.at[position].set(grad_values.astype(jnp.bfloat16))
    back_keys, back_values = (
        lax.all_to_all(outgoing_keys, "st", split_axis=0, concat_axis=0, tiled=True),
        lax.all_to_all(outgoing_values, "st", split_axis=0, concat_axis=0, tiled=True),
    )
    asked_flat = asked_ids.reshape(-1)
    owner_pick = (asked_flat[None, :] == jnp.arange(passages, dtype=jnp.int32)[:, None]).astype(
        jnp.bfloat16
    )
    passage_keys = jnp.dot(
        owner_pick,
        back_keys.reshape(st_size * slot_cap, passage_len * local_width),
        preferred_element_type=jnp.float32,
    )
    passage_values = jnp.dot(
        owner_pick,
        back_values.reshape(st_size * slot_cap, passage_len * local_width),
        preferred_element_type=jnp.float32,
    )
    passage_keys = passage_keys.astype(jnp.bfloat16).reshape(rows_dev, local_width)
    passage_values = passage_values.astype(jnp.bfloat16).reshape(rows_dev, local_width)
    weight_terms = lax.dot_general(
        normed, passage_values, (((0,), (0,)), ((), ())), preferred_element_type=jnp.float32
    )
    grad_w_value = lax.psum_scatter(weight_terms, "st", scatter_dimension=0, tiled=True)
    quarter = rows_dev // tp_size
    whole_key, whole_value = (
        lax.all_gather(w_key, "tp", axis=1, tiled=True),
        lax.all_gather(w_value, "tp", axis=1, tiled=True),
    )
    own_keys, own_values = (
        lax.all_to_all(passage_keys, "tp", split_axis=0, concat_axis=1, tiled=True),
        lax.all_to_all(passage_values, "tp", split_axis=0, concat_axis=1, tiled=True),
    )
    grad_normed = contract(own_keys, whole_key) + contract(own_values, whole_value)
    first_row = lax.axis_index("tp") * quarter
    own_rows = lax.dynamic_slice_in_dim(store_rows, first_row, quarter, 0)
    own_inverse = lax.dynamic_slice_in_dim(row_inverse, first_row, quarter, 0)
    unit_rows = own_rows * own_inverse
    grad_unit = grad_normed * store_gain
    grad_store = own_inverse * (
        grad_unit - unit_rows * jnp.mean(grad_unit * unit_rows, axis=-1, keepdims=True)
    )
    return (grad_queries, grad_store, grad_w_value)


FAR = -1e30
MESH = pl.DeviceIdType.MESH


def place_of(index, n):
    odd = index % 2
    return (1 - odd) * (index // 2) + odd * (n - 1 - index // 2)


def index_at(place, n):
    place = (place + 2 * n) % n
    back = place // (n // 2)
    return (1 - back) * (2 * place) + back * (2 * (n - 1 - place) + 1)


def greet(others):
    barrier = pltpu.get_barrier_semaphore()
    for axis, other in others:
        pl.semaphore_signal(barrier, inc=1, device_id={axis: other}, device_id_type=MESH)
    pl.semaphore_wait(barrier, len(others))


def gather_kernel(n, q_ref, g_ref, i_ref, x_ref, gain_ref, wk_ref, wv_ref, q_all, g_all, i_all, normed_ref, kt_ref, vt_ref, send_sem, recv_sem, own_sem):
    me = lax.axis_index("st")
    place = place_of(me, n)
    right, left = index_at(place + 1, n), index_at(place - 1, n)
    half_rows = q_ref.shape[0] // 2
    pairs = ((q_ref, q_all), (g_ref, g_all), (i_ref, i_all))
    greet((("st", left), ("st", right)))
    own = []
    for number, (src, dst) in enumerate(pairs):
        copy = pltpu.make_async_copy(src, dst.at[me], own_sem.at[number])
        copy.start()
        own.append(copy)
    hops = n // 2
    parts = ((2, 0), (0, 0), (0, 1), (1, 0), (1, 1))

    def last_on(side, part):
        return parts[part][1] == side

    def piece(side, step, part):
        number, half = parts[part]
        src, dst = pairs[number]
        origin = index_at(place - step, n) if side == 0 else index_at(place + step, n)
        rows = pl.ds(0, i_ref.shape[0]) if number == 2 else pl.ds(half * half_rows, half_rows)
        return pltpu.make_async_remote_copy(
            src_ref=src.at[rows] if step == 0 else dst.at[origin, rows],
            dst_ref=dst.at[origin, rows],
            send_sem=send_sem.at[side, step, part],
            recv_sem=recv_sem.at[side, step, part],
            device_id={"st": right if side == 0 else left},
            device_id_type=MESH,
        )

    count = x_ref.shape[0] // 128

    def project(chunk):
        rows = pl.ds(chunk * 128, 128)
        wide = x_ref[rows].astype(jnp.float32)
        normed = (wide * row_scale(wide) * gain_ref[...]).astype(jnp.bfloat16)
        normed_ref[rows] = normed
        kt_ref[rows] = jnp.dot(normed, wk_ref[...], preferred_element_type=jnp.float32).astype(jnp.bfloat16)
        vt_ref[rows] = jnp.dot(normed, wv_ref[...], preferred_element_type=jnp.float32).astype(jnp.bfloat16)

    chunk = 0
    started = []
    for step in range(hops):
        for part in range(5):
            for side in range(2):
                if step < hops - 1 or last_on(side, part):
                    if step > 0:
                        piece(side, step - 1, part).wait_recv()
                    copy = piece(side, step, part)
                    copy.start()
                    started.append(copy)
            if part > 0 and chunk < count:
                project(chunk)
                chunk += 1
    for rest in range(chunk, count):
        project(rest)
    for part in range(5):
        for side in range(2):
            if not last_on(side, part):
                piece(side, hops - 2, part).wait_recv()
    for part in range(5):
        piece(parts[part][1], hops - 1, part).wait_recv()
    for copy in own:
        copy.wait()
    for copy in started:
        copy.wait_send()


def ring_gather(queries, grad_in, named, store, gain, w_key, w_value, n):
    hops = n // 2
    vmem = pl.BlockSpec(memory_space=pltpu.VMEM)
    sources = (queries, grad_in, named)
    return pl.pallas_call(
        functools.partial(gather_kernel, n),
        out_shape=tuple(jax.ShapeDtypeStruct((n,) + x.shape, x.dtype) for x in sources)
        + (jax.ShapeDtypeStruct(store.shape, jnp.bfloat16),)
        + (jax.ShapeDtypeStruct((store.shape[0], w_key.shape[1]), jnp.bfloat16),) * 2,
        in_specs=[vmem] * 7,
        out_specs=(vmem,) * 6,
        scratch_shapes=[
            pltpu.SemaphoreType.DMA((2, hops, 5)),
            pltpu.SemaphoreType.DMA((2, hops, 5)),
            pltpu.SemaphoreType.DMA((3,)),
        ],
        cost_estimate=pl.CostEstimate(flops=10**10, bytes_accessed=10**7, transcendentals=0),
        compiler_params=pltpu.CompilerParams(collective_id=0, has_side_effects=True, vmem_limit_bytes=40 << 20),
        name="ring_gather",
    )(*sources, store, gain[None], w_key, w_value)


def join_kernel(n, heads, x_ref, out_ref, got, mine, send_sem, recv_sem, own_sem):
    me = lax.axis_index("st")
    peers = [(me + away) % n for away in range(1, n)]
    greet([("st", peer) for peer in peers])

    def piece(phase, away):
        peer = (me + away) % n
        return pltpu.make_async_remote_copy(
            src_ref=x_ref.at[peer] if phase == 0 else mine,
            dst_ref=got.at[me] if phase == 0 else out_ref.at[me],
            send_sem=send_sem.at[phase, away],
            recv_sem=recv_sem.at[phase, away],
            device_id={"st": peer},
            device_id_type=MESH,
        )

    for away in range(1, n):
        piece(0, away).start()
    local = pltpu.make_async_copy(x_ref.at[me], got.at[me], own_sem.at[0])
    local.start()
    local.wait()
    for away in range(1, n):
        piece(0, away).wait()
    for head in range(heads):
        logs = [got[owner, :, 2 * head] for owner in range(n)]
        top = functools.reduce(jnp.maximum, logs)
        shares = [jnp.exp(one - top) for one in logs]
        total = sum(shares)
        mine[:, 2 * head] = top + jnp.log(total)
        mine[:, 2 * head + 1] = sum(share * got[owner, :, 2 * head + 1] for owner, share in enumerate(shares)) / total
    out_ref[me] = mine[...]
    for away in range(1, n):
        piece(1, away).start()
    for away in range(1, n):
        piece(1, away).wait()


def join_stats(stats, n):
    total, rows, width = stats.shape
    blocks = total // n
    vmem = pl.BlockSpec(memory_space=pltpu.VMEM)
    joined = pl.pallas_call(
        functools.partial(join_kernel, n, rows // 2),
        out_shape=jax.ShapeDtypeStruct((n, blocks, rows, width), jnp.float32),
        in_specs=[vmem],
        out_specs=vmem,
        scratch_shapes=[
            pltpu.VMEM((n, blocks, rows, width), jnp.float32),
            pltpu.VMEM((blocks, rows, width), jnp.float32),
            pltpu.SemaphoreType.DMA((2, n)),
            pltpu.SemaphoreType.DMA((2, n)),
            pltpu.SemaphoreType.DMA((1,)),
        ],
        cost_estimate=pl.CostEstimate(flops=10**9, bytes_accessed=10**6, transcendentals=0),
        compiler_params=pltpu.CompilerParams(collective_id=2, has_side_effects=True),
        name="join_stats",
    )(stats.reshape(n, blocks, rows, width))
    return joined.reshape(total, rows, width)


def scatter_kernel(n, tp, parts, x_ref, w_ref, k_ref, v_ref, out_ref, gw_ref, ok_ref, ov_ref, send_buf, recv_buf, send_sem, recv_sem, tp_send, tp_recv, own_sem):
    me = lax.axis_index("st")
    mine = lax.axis_index("tp")
    place = place_of(me, n)
    right, left = index_at(place + 1, n), index_at(place - 1, n)
    tokens = x_ref.shape[1]
    greet([("st", left), ("st", right)] + [("tp", (mine + away) % tp) for away in range(1, tp)])
    quarter, width = ok_ref.shape[0], k_ref.shape[1]
    columns = pl.ds(pl.multiple_of(mine * width, 128), width)

    def across(number, away):
        src, dst = ((k_ref, ok_ref), (v_ref, ov_ref))[number]
        peer = (mine + away) % tp
        return pltpu.make_async_remote_copy(
            src_ref=src.at[pl.ds(pl.multiple_of(peer * quarter, 16), quarter)],
            dst_ref=dst.at[:, columns],
            send_sem=tp_send.at[number, away],
            recv_sem=tp_recv.at[number, away],
            device_id={"tp": peer},
            device_id_type=MESH,
        )

    def kept(number):
        src, dst = ((k_ref, ok_ref), (v_ref, ov_ref))[number]
        return pltpu.make_async_copy(
            src.at[pl.ds(pl.multiple_of(mine * quarter, 16), quarter)], dst.at[:, columns], own_sem.at[number]
        )

    for number in range(2):
        kept(number).start()
        for away in range(1, tp):
            across(number, away).start()
    hops = n // 2

    def used(side, step, part):
        return step > 0 or parts[part][3] == side

    def piece(side, step, part):
        number, first, count, _ = parts[part]
        at = pl.ds(number * tokens + first, count)
        return pltpu.make_async_remote_copy(
            src_ref=send_buf.at[side, step, at],
            dst_ref=recv_buf.at[side, step, at],
            send_sem=send_sem.at[side, step, part],
            recv_sem=recv_sem.at[side, step, part],
            device_id={"st": right if side == 0 else left},
            device_id_type=MESH,
        )

    started = []
    for step in range(hops):
        for part, (number, first, count, _) in enumerate(parts):
            for side in range(2):
                if not used(side, step, part):
                    continue
                distance = hops - step
                dest = index_at(place + distance, n) if side == 0 else index_at(place - distance, n)
                at = pl.ds(number * tokens + first, count)
                total = (x_ref, w_ref)[number][dest, pl.ds(first, count)]
                if step > 0 and used(side, step - 1, part):
                    piece(side, step - 1, part).wait_recv()
                    total = (total.astype(jnp.float32) + recv_buf[side, step - 1, at].astype(jnp.float32)).astype(jnp.bfloat16)
                send_buf[side, step, at] = total
                copy = piece(side, step, part)
                copy.start()
                started.append(copy)
    for part, (number, first, count, _) in enumerate(parts):
        at = pl.ds(number * tokens + first, count)
        total = (x_ref, w_ref)[number][me, pl.ds(first, count)].astype(jnp.float32)
        for side in range(2):
            piece(side, hops - 1, part).wait_recv()
            total = total + recv_buf[side, hops - 1, at].astype(jnp.float32)
        (out_ref, gw_ref)[number][pl.ds(first, count)] = total
    for number in range(2):
        kept(number).wait()
        for away in range(1, tp):
            across(number, away).wait()
    for copy in started:
        copy.wait_send()


def ring_scatter(terms, weight_terms, keys, values, n, tp):
    rows, width = terms.shape[1:]
    rest = weight_terms.shape[1]
    hops = n // 2
    parts = ((0, 0, rows // 4, 0), (0, rows // 2, rows // 4, 1), (0, rows // 4, rows // 4, 0),
             (0, 3 * rows // 4, rows // 4, 1), (1, 0, rest // 2, 0), (1, rest // 2, rest // 2, 1))
    vmem = pl.BlockSpec(memory_space=pltpu.VMEM)
    own = jax.ShapeDtypeStruct((keys.shape[0] // tp, width * tp), jnp.bfloat16)
    return pl.pallas_call(
        functools.partial(scatter_kernel, n, tp, parts),
        out_shape=(
            jax.ShapeDtypeStruct((rows, width), jnp.float32),
            jax.ShapeDtypeStruct((rest, width), jnp.float32),
            own,
            own,
        ),
        in_specs=[vmem] * 4,
        out_specs=(vmem,) * 4,
        scratch_shapes=[
            pltpu.VMEM((2, hops, rows + rest, width), jnp.bfloat16),
            pltpu.VMEM((2, hops, rows + rest, width), jnp.bfloat16),
            pltpu.SemaphoreType.DMA((2, hops, len(parts))),
            pltpu.SemaphoreType.DMA((2, hops, len(parts))),
            pltpu.SemaphoreType.DMA((2, tp)),
            pltpu.SemaphoreType.DMA((2, tp)),
            pltpu.SemaphoreType.DMA((2,)),
        ],
        cost_estimate=pl.CostEstimate(flops=5 * 10**9, bytes_accessed=10**7, transcendentals=0),
        compiler_params=pltpu.CompilerParams(collective_id=1, has_side_effects=True, vmem_limit_bytes=50 << 20),
        name="ring_scatter",
    )(terms, weight_terms, keys, values)


NT = (((1,), (1,)), ((), ()))
TN = (((0,), (0,)), ((), ()))


def dot(left, right, dims=(((1,), (0,)), ((), ()))):
    return lax.dot_general(left, right, dims, preferred_element_type=jnp.float32)


def items_of(table, total, heads, turn):
    items = []
    for lane in range(2):
        block = table[total + 2 * turn + lane]
        picked = table[block]
        for head in range(heads):
            items.append((block, picked >= 0, jnp.maximum(picked, 0), head, pl.ds(head * HD, HD)))
    return items


def raw_products(items, q_ref, g_ref, k_ref, v_ref):
    scale = HD ** (-0.5)
    scores = [dot(k_ref[picked, :, cols], q_ref[block, :, cols], NT) * scale for block, _, picked, _, cols in items]
    grads = [dot(v_ref[picked, :, cols], g_ref[block, :, cols], NT) for block, _, picked, _, cols in items]
    return scores, grads


def stats_kernel(heads, table, q_ref, g_ref, k_ref, v_ref, out_ref):
    total, _, block_len = out_ref.shape

    @pl.loop(0, total)
    def _(block):
        for head in range(heads):
            out_ref[block, 2 * head] = jnp.full((block_len,), FAR, jnp.float32)
            out_ref[block, 2 * head + 1] = jnp.zeros((block_len,), jnp.float32)

    @pl.loop(0, (table[2 * total] + 1) // 2)
    def _(turn):
        items = items_of(table, total, heads, turn)
        scores, grads = raw_products(items, q_ref, g_ref, k_ref, v_ref)
        tops = [jnp.max(one, axis=0, keepdims=True) for one in scores]
        raised = [jnp.exp(one - top) for one, top in zip(scores, tops)]
        totals = [jnp.sum(one, axis=0, keepdims=True) for one in raised]
        means = [jnp.sum(one * two, axis=0, keepdims=True) / three for one, two, three in zip(raised, grads, totals)]
        logs = [top + jnp.log(one) for top, one in zip(tops, totals)]
        for number, (block, live, _, head, _) in enumerate(items):
            @pl.when(live)
            def _():
                out_ref[block, pl.ds(2 * head, 1)] = logs[number]
                out_ref[block, pl.ds(2 * head + 1, 1)] = means[number]


def grads_kernel(heads, table, q_ref, g_ref, k_ref, v_ref, s_ref, dq_ref, pk_ref, pv_ref, dk_acc, dv_acc):
    scale = HD ** (-0.5)
    total = dq_ref.shape[0]
    dk_acc[...] = jnp.zeros_like(dk_acc)
    dv_acc[...] = jnp.zeros_like(dv_acc)

    @pl.loop(table[2 * total], total)
    def _(at):
        dq_ref[table[total + at]] = jnp.zeros(dq_ref.shape[1:], jnp.bfloat16)

    @pl.loop(0, (table[2 * total] + 1) // 2)
    def _(turn):
        items = items_of(table, total, heads, turn)
        scores, grads = raw_products(items, q_ref, g_ref, k_ref, v_ref)
        weights, halves = [], []
        for (block, _, _, head, _), score, grad in zip(items, scores, grads):
            weight = jnp.exp(score - s_ref[block, pl.ds(2 * head, 1)])
            halves.append((weight * (grad - s_ref[block, pl.ds(2 * head + 1, 1)])).astype(jnp.bfloat16))
            weights.append(weight.astype(jnp.bfloat16))
        steps, keys, values = [], [], []
        for (block, _, picked, _, cols), weight, half in zip(items, weights, halves):
            keys.append(dot(half, q_ref[block, :, cols]) * scale)
            values.append(dot(weight, g_ref[block, :, cols]))
            steps.append((dot(half, k_ref[picked, :, cols], TN) * scale).astype(jnp.bfloat16))
        for number, (block, live, picked, _, cols) in enumerate(items):
            @pl.when(live)
            def _():
                dq_ref[block, :, cols] = steps[number]
                dk_acc[picked, :, cols] += keys[number]
                dv_acc[picked, :, cols] += values[number]

    pk_ref[...] = dk_acc[...].astype(jnp.bfloat16)
    pv_ref[...] = dv_acc[...].astype(jnp.bfloat16)


def table_of(ids):
    total = ids.shape[0]
    spot = jnp.arange(total, dtype=jnp.int32)
    idle = (ids < 0).astype(jnp.int32)
    sort_key = idle * total + spot
    rank = jnp.sum((sort_key[None, :] < sort_key[:, None]).astype(jnp.int32), axis=1)
    order = jnp.sum(jnp.where(rank[None, :] == spot[:, None], spot[None, :], 0), axis=1)
    count = total - jnp.sum(idle)
    return jnp.concatenate([ids, order, count[None]])


def query_plan(queries, gate_pre, cotangent, store, store_gain, w_key, w_value, owners, slots):
    n = lax.axis_size("st")
    tp_size = lax.axis_size("tp")
    me = lax.axis_index("st")
    blocks, per_block = owners.shape
    tok_rows, local_width = queries.shape
    heads = local_width // HD
    block_len = tok_rows // blocks
    rows_dev = store.shape[0]
    passages = rows_dev // PLEN
    named = jnp.pad(owners * passages + slots, ((0, 0), (0, 128 - per_block)), constant_values=-1)
    gate_open = jax.nn.sigmoid(gate_pre.astype(jnp.float32))
    grad_in = (gate_open * cotangent.astype(jnp.float32)).astype(jnp.bfloat16)
    q_all, g_all, all_named, normed, key_table, value_table = ring_gather(
        queries, grad_in, named, store, store_gain, w_key, w_value, n
    )
    held = all_named.reshape(n * blocks, 128)[:, :per_block] - me * passages
    ids = jnp.max(jnp.where((held >= 0) & (held < passages), held, -1), axis=1)
    key_table = key_table.reshape(passages, PLEN, local_width)
    value_table = value_table.reshape(passages, PLEN, local_width)
    table = table_of(ids)
    total = n * blocks
    q_blocks = q_all.reshape(total, block_len, local_width)
    g_blocks = g_all.reshape(total, block_len, local_width)
    smem = pl.BlockSpec(memory_space=pltpu.SMEM)
    vmem = pl.BlockSpec(memory_space=pltpu.VMEM)
    stats = pl.pallas_call(
        functools.partial(stats_kernel, heads),
        out_shape=jax.ShapeDtypeStruct((total, 2 * heads, block_len), jnp.float32),
        in_specs=[smem] + [vmem] * 4,
        out_specs=vmem,
        compiler_params=pltpu.CompilerParams(vmem_limit_bytes=40 << 20),
        name="stats",
    )(table, q_blocks, g_blocks, key_table, value_table)
    joined = join_stats(stats, n)
    dq, passage_keys, passage_values = pl.pallas_call(
        functools.partial(grads_kernel, heads),
        out_shape=(
            jax.ShapeDtypeStruct((total, block_len, local_width), jnp.bfloat16),
            jax.ShapeDtypeStruct((passages, PLEN, local_width), jnp.bfloat16),
            jax.ShapeDtypeStruct((passages, PLEN, local_width), jnp.bfloat16),
        ),
        in_specs=[smem] + [vmem] * 5,
        out_specs=(vmem,) * 3,
        scratch_shapes=[pltpu.VMEM((passages, PLEN, local_width), jnp.float32)] * 2,
        compiler_params=pltpu.CompilerParams(vmem_limit_bytes=40 << 20),
        name="grads",
    )(table, q_blocks, g_blocks, key_table, value_table, joined)
    dq = dq.reshape(n, tok_rows, local_width)
    passage_keys = passage_keys.reshape(rows_dev, local_width)
    passage_values = passage_values.reshape(rows_dev, local_width)
    weight_terms = lax.dot_general(
        normed, passage_values, (((0,), (0,)), ((), ())), preferred_element_type=jnp.float32
    ).astype(jnp.bfloat16)
    whole_key, whole_value = (
        lax.all_gather(w_key, "tp", axis=1, tiled=True),
        lax.all_gather(w_value, "tp", axis=1, tiled=True),
    )
    quarter = rows_dev // tp_size
    grad_queries, grad_w_value, own_keys, own_values = ring_scatter(
        dq, weight_terms.reshape(n, -1, local_width), passage_keys, passage_values, n, tp_size
    )
    grad_normed = contract(own_keys, whole_key) + contract(own_values, whole_value)
    first_row = lax.axis_index("tp") * quarter
    own_rows = lax.dynamic_slice_in_dim(store, first_row, quarter, 0).astype(jnp.float32)
    own_inverse = row_scale(own_rows)
    unit_rows = own_rows * own_inverse
    grad_unit = grad_normed * store_gain
    grad_store = own_inverse * (
        grad_unit - unit_rows * jnp.mean(grad_unit * unit_rows, axis=-1, keepdims=True)
    )
    return (grad_queries, grad_store, grad_w_value)


def local(*arrays):
    queries, owners = arrays[0], arrays[7]
    n = lax.axis_size("st")
    slot_cap = (2 * owners.size + n - 1) // n
    if n % 2 == 0 and n >= 4 and 8 * slot_cap * PLEN >= 3 * queries.shape[0]:
        return query_plan(*arrays)
    return passage_plan(*arrays)


def solution(mesh):
    placed = (
        P("st", "tp"),
        P("st", "tp"),
        P("st", "tp"),
        P("st", None),
        P(),
        P(None, "tp"),
        P(None, "tp"),
        P("st", None),
        P("st", None),
    )
    return jax.shard_map(
        local,
        mesh=mesh,
        in_specs=placed,
        out_specs=(P("st", "tp"), P(("st", "tp"), None), P("st", "tp")),
        check_vma=False,
    )
```

profile of v0, /device:TPU:0, one launch (start us, length us, event | category | flops | bytes accessed | tf_op | source)
XLA Modules:
  0.0 245.1 jit_solution(10757542216413291179)
XLA Ops:
  7.2 0.0 copy-start.5
  7.2 0.0 copy-start.6
  7.2 0.0 copy-start.11
  7.2 0.0 all-gather.3.cloned.1.call-start
  7.2 0.7 all-gather.3.cloned.1.call-update
  7.9 0.0 all-gather.5.cloned.1.call-start
  8.0 0.7 all-gather.5.cloned.1.call-update
  8.7 0.8 copy.14
  9.4 0.8 copy.15
  10.2 1.5 multiply_convert_fusion.g_ref
  11.7 0.0 copy-done.5
  11.7 0.0 copy-done.6
  11.7 0.0 copy-done.11
  11.8 0.0 copy-start.10
  11.8 1.0 copy-done.10
  12.8 89.7 %ring_gather.1 = (bf16[8,1024,256]{2,1,0:T(8,128)(2,1)S(1)}, bf16[8,1024,256]{2,1,0:T(8,128)(2,1)S(1)}, s32[8,8,128]{2,1,0:T(8,128)S(1)}, bf16[1280,2048]{1,0:T(...) custom-call(bf16[1024,256]{1,0:T(8,128)(2,1)S(1)} %copy-done.10, ...), custom_call_target="tpu_custom_call" | custom-call | flops 10000000000 | bytes 10000000 | tf_op jit(solution)/shard_map/ring_gather/pallas_call | solution.py:256
  102.5 0.0 copy-start
  102.5 2.0 copy-done
  104.5 1.9 copy-done.3
  106.4 0.1 select_reduce_fusion.1
  106.5 0.6 fusion.7
  107.8 0.2 convert_reduce_fusion
  108.0 0.1 select_reduce_fusion
  108.1 0.1 pad_add_fusion.table
  108.2 0.0 copy-start.1
  108.2 2.2 copy-done.1
  110.4 2.2 copy-done.4
  112.6 3.3 %stats.1 = f32[64,4,128]{2,1,0:T(4,128)S(1)} custom-call(s32[129]{0:T(256)S(1)} %pad_add_fusion.table, bf16[64,128,256]{2,1,0:T(8,128)(2,1)S(1)} %bitcast.19, bf16[64,128,256]{2,1,0:T(8,128)(2,1)S(1)} %bitcast.22, bf16[20,64,256]{2,1,0:T(8,128)(2,1)S(1)} %bitcast.23, bf16[20,64,256]{2,1,0:T(8,128)(2,1)S(1)} %bitcast.25), custom_call_target="tpu_custom_call" | custom-call | tf_op jit(solution)/shard_map/stats/pallas_call | solution.py:570
  115.8 0.0 copy-start.8
  115.8 0.6 copy-done.8
  116.5 20.9 %join_stats.1 = f32[8,8,4,128]{3,2,1,0:T(4,128)} custom-call(f32[8,8,4,128]{3,2,1,0:T(4,128)} %bitcast.28), custom_call_target="tpu_custom_call" | custom-call | flops 1000000000 | bytes 1000000 | tf_op jit(solution)/shard_map/join_stats/pallas_call | solution.py:315
  137.4 0.0 copy-start.2
  137.4 2.2 copy-done.2
  139.6 0.9 copy-done.7
  140.5 7.7 %grads.1 = (bf16[64,128,256]{2,1,0:T(8,128)(2,1)S(1)}, bf16[20,64,256]{2,1,0:T(8,128)(2,1)S(1)}, bf16[20,64,256]{2,1,0:T(8,128)(2,1)S(1)}) custom-call(s32[129]{0:T(256)S(1)} %pad_add_fusion.table, bf16[64,128,256]{2,1,0:T(8,128)(2,1)S(1)} %bitcast.20, bf16[64,128,256]{2,1,0:T(8,128)(2,1)} %bitcast.21, bf16[20,64,256]{2,1,0:T(8,128)(2,1)S(1)} %bitcast.24, ...), custom_call_target="tpu_custom_call" | custom-call | tf_op jit(solution)/shard_map/grads/pallas_call | solution.py:579
  148.2 0.0 copy-start.9
  148.2 1.9 copy-done.9
  150.1 5.1 %convolution_convert_fusion = bf16[2048,256]{1,0:T(8,128)(2,1)} fusion(bf16[1280,2048]{1,0:T(8,128)(2,1)} %get-tuple-element.22, bf16[1280,256]{1,0:T(8,128)(2,1)S(1)} %bitcast.32), kind=kOutput, calls=%fused_computation.10 | convolution fusion | flops 1342701568 | bytes 6946816 | tf_op jit(solution)/shard_map/dot_general | solution.py:595
  155.2 64.9 %ring_scatter.1 = (f32[1024,256]{1,0:T(8,128)S(1)}, f32[256,256]{1,0:T(8,128)S(1)}, bf16[320,1024]{1,0:T(8,128)(2,1)S(1)}, bf16[320,1024]{1,0:T(8,128)(2,1)S(1)}) custom-call(bf16[8,1024,256]{2,1,0:T(8,128)(2,1)} %bitcast.30, bf16[8,256,256]{2,1,0:T(8,128)(2,1)} %bitcast.35, bf16[1280,256]{1,0:T(8,128)(2,1)S(1)} %bitcast.31, bf16[1280,256]{1,0:T(8,128)(2,1)S(1)} %bitcast.33), custom_call_target="tpu_custom_call" | custom-call | flops 5000000000 | bytes 10000000 | tf_op jit(solution)/shard_map/ring_scatter/pallas_call | solution.py:423
  220.1 0.0 copy-start.12
  220.1 0.8 copy-done.12
  220.9 1.7 fusion.6
  222.6 0.0 all-gather.3.cloned.1.call-done
  222.6 5.5 %fusion.9 = f32[320,2048]{1,0:T(8,128)} fusion(bf16[320,1024]{1,0:T(8,128)(2,1)} %copy-done.12, bf16[2048,1024]{1,0:T(8,128)(2,1)} %all-gather.3.cloned.1.call-done), kind=kOutput, calls=%fused_computation.25 | convolution fusion | flops 1342177280 | bytes 7471104 | tf_op jit(solution)/shard_map/dot_general | solution.py:22
  228.1 5.2 %fusion.3 = (f32[320]{0:T(512)S(1)}, f32[320,2048]{1,0:T(8,128)S(1)}) fusion(f32[320]{0:T(512)S(1)} %add_rsqrt_fusion, bf16[1280,2048]{1,0:T(8,128)(2,1)} %x_ref.1, s32[]{:T(128)S(6)} %select_n.13, f32[2048]{0:T(1024)S(1)} %copy-done.11, f32[320,2048]{1,0:T(8,128)} %fusion.9, bf16[320,1024]{1,0:T(8,128)(2,1)S(1)} %get-tuple-element.27, ...), kind=kOutput, calls=%fused_computation.6 | convolution fusion | flops 1346109184 | bytes 11414020 | tf_op jit(solution)/shard_map/dot_general | solution.py:22
  233.3 3.3 %fusion.5 = f32[320,2048]{1,0:T(8,128)} fusion(f32[320,2048]{1,0:T(8,128)S(1)} %get-tuple-element.32, f32[320]{0:T(512)S(1)} %broadcast_multiply_fusion, f32[320]{0:T(512)S(1)} %add_rsqrt_fusion, bf16[1280,2048]{1,0:T(8,128)(2,1)} %x_ref.1, s32[]{:T(128)S(6)} %select_n.13), kind=kLoop, calls=%fused_computation.8 | loop fusion | flops 3276800 | bytes 6556164 | tf_op jit(solution)/shard_map/mul | solution.py:612
  236.6 1.0 copy.18
  237.6 0.7 copy.19
  (8 shorter events, 0.0 us)
Async XLA Ops:
  7.2 4.6 %copy-start.5 = (bf16[2048,256]{1,0:T(8,128)(2,1)S(1)}, bf16[2048,256]{1,0:T(8,128)(2,1)}, u32[]{:S(2)}) copy-start(bf16[2048,256]{1,0:T(8,128)(2,1)} %wk_ref.1) | copy-start | bytes 3145732
  7.2 4.6 %copy-start.6 = (bf16[2048,256]{1,0:T(8,128)(2,1)S(1)}, bf16[2048,256]{1,0:T(8,128)(2,1)}, u32[]{:S(2)}) copy-start(bf16[2048,256]{1,0:T(8,128)(2,1)} %wv_ref.1) | copy-start | bytes 3145732
  7.2 4.6 %copy-start.11 = (f32[2048]{0:T(1024)S(1)}, f32[2048]{0:T(1024)}, u32[]{:S(2)}) copy-start(f32[2048]{0:T(1024)} %param.13) | copy-start | bytes 24580
  7.2 215.4 %all-gather.3.cloned.1.call-start = ((), (), s32[]{:S(2)}) async-start(), calls=%async_computation | async-start | bytes 5242880 | tf_op jit(solution)/shard_map/all_gather | solution.py:599
  7.9 220.1 %all-gather.5.cloned.1.call-start = ((), (), s32[]{:S(2)}) async-start(), calls=%async_computation.1 | async-start | bytes 5242880 | tf_op jit(solution)/shard_map/all_gather | solution.py:600
  11.8 1.0 copy-start.10
  102.5 2.0 copy-start
  104.5 1.9 copy-start.3
  108.2 2.2 copy-start.1
  110.4 2.2 copy-start.4
  115.8 0.7 copy-start.8
  137.4 2.2 copy-start.2
  139.6 0.9 copy-start.7
  148.2 1.9 copy-start.9
  220.1 0.8 copy-start.12
Sparse Core Ops, SparseCore 0:
  9.6 37.7 all-gather.2
  48.9 34.9 all-gather.4
where the time goes:
time: 248 us; the launch traced here: 245 us
  Pallas kernels  186 us (75%)
  local copies, waits for them, and re-layouts  19.1 us (8%)
  matrix products  15.7 us (6%)
  between operations  14.9 us (6%)
  other arithmetic  7.64 us (3%)
    pallas_call x1, Pallas kernels, ring_gather(): pl.pallas_call(functools.partial(gather_kernel, n), out_shape=tuple((jax....  89.7 us
    pallas_call x1, Pallas kernels, ring_scatter(): pl.pallas_call(functools.partial(scatter_kernel, n, tp, parts), out_shape...  64.9 us
    pallas_call x1, Pallas kernels, join_stats(): pl.pallas_call(functools.partial(join_kernel, n, rows // 2), out_shape=ja...  20.9 us
    unnamed x30, local copies, waits for them, and re-layouts  19.1 us
    dot_general x2, matrix products, contract(): lax.dot_general(left, right, (((1,), (1,)), ((), ())), preferred_element_...  10.6 us
    pallas_call x1, Pallas kernels, query_plan(): pl.pallas_call(functools.partial(grads_kernel, heads), out_shape=(jax.Sha...  7.66 us
    dot_general x1, matrix products, query_plan(): lax.dot_general(normed, passage_values, (((0,), (0,)), ((), ())), preferr...  5.08 us
  transfers between devices with their start and end apart: 2, of which 0 were waited for; matrix products, arithmetic and copies ran while one was open for 7% of the time, Pallas kernels for 76%

commit v1 on v0

v1 whole, which is shorter than its diff:
```python
import functools

import jax
import jax.numpy as jnp
from jax import lax
from jax.experimental import pallas as pl
from jax.experimental.pallas import tpu as pltpu
from jax.sharding import PartitionSpec as P

HD = 128
PLEN = 64


EPS = 1e-06


def row_scale(store_rows):
    return lax.rsqrt(jnp.mean(store_rows * store_rows, axis=-1, keepdims=True) + EPS)


def contract(left, right):
    return lax.dot_general(
        left, right, (((1,), (1,)), ((), ())), preferred_element_type=jnp.float32
    )


def passage_plan(queries, gate_pre, cotangent, store, store_gain, w_key, w_value, owners, slots):
    st_size = lax.axis_size("st")
    tp_size = lax.axis_size("tp")
    blocks, per_block = owners.shape
    tok_rows, local_width = queries.shape
    head_dim = HD
    local_heads = local_width // head_dim
    block_len = tok_rows // blocks
    passage_len = PLEN
    rows_dev = store.shape[0]
    passages = rows_dev // passage_len
    slot_count = blocks * per_block
    slot_cap = (2 * slot_count + st_size - 1) // st_size
    store_rows = store.astype(jnp.float32)
    row_inverse = row_scale(store_rows)
    normed = (store_rows * row_inverse * store_gain).astype(jnp.bfloat16)
    key_table = jnp.dot(normed, w_key, preferred_element_type=jnp.float32).astype(jnp.bfloat16)
    value_table = jnp.dot(normed, w_value, preferred_element_type=jnp.float32).astype(jnp.bfloat16)
    key_table = key_table.reshape(passages, passage_len, local_width)
    value_table = value_table.reshape(passages, passage_len, local_width)
    owner_flat = owners.reshape(slot_count)
    slot_flat = slots.reshape(slot_count)
    slot_order = jnp.arange(slot_count, dtype=jnp.int32)
    earlier_same = (owner_flat[:, None] == owner_flat[None, :]) & (
        slot_order[None, :] < slot_order[:, None]
    )
    slot_rank = jnp.sum(earlier_same.astype(jnp.int32), axis=1)
    position = owner_flat * slot_cap + slot_rank
    places = jnp.arange(st_size * slot_cap, dtype=jnp.int32)
    slot_hits = position[:, None] == places[None, :]
    requests = jnp.sum(jnp.where(slot_hits, slot_flat[:, None], 0), axis=0)
    requests = requests.reshape(st_size, slot_cap)
    asked_ids = lax.all_to_all(requests, "st", split_axis=0, concat_axis=0, tiled=True)
    asked_flat = asked_ids.reshape(-1)
    shape_out = asked_ids.shape + (passage_len, local_width)
    picked_keys = jnp.take(key_table, asked_flat, axis=0).reshape(shape_out)
    picked_values = jnp.take(value_table, asked_flat, axis=0).reshape(shape_out)
    sent_keys = lax.all_to_all(picked_keys, "st", split_axis=0, concat_axis=0, tiled=True)
    sent_values = lax.all_to_all(picked_values, "st", split_axis=0, concat_axis=0, tiled=True)
    got_keys, got_values, asked_ids = (sent_keys, sent_values, asked_ids)
    span = per_block * passage_len
    mine_keys = jnp.take(
        got_keys.reshape(st_size * slot_cap, passage_len, local_width), position, axis=0
    )
    mine_values = jnp.take(
        got_values.reshape(st_size * slot_cap, passage_len, local_width), position, axis=0
    )
    mine_keys = mine_keys.reshape(blocks, span, local_heads, head_dim)
    mine_values = mine_values.reshape(blocks, span, local_heads, head_dim)
    score_scale = head_dim ** (-0.5)
    query_blocks = queries.reshape(blocks, block_len, local_heads, head_dim)
    gate_open = jax.nn.sigmoid(gate_pre.astype(jnp.float32))
    grad_in = (gate_open * cotangent.astype(jnp.float32)).astype(jnp.bfloat16)
    grad_in = grad_in.reshape(blocks, block_len, local_heads, head_dim)
    scores = (
        jnp.einsum("bqhd,bkhd->bhqk", query_blocks, mine_keys, preferred_element_type=jnp.float32)
        * score_scale
    )
    shifted = scores - jnp.max(scores, axis=-1, keepdims=True)
    weights = jnp.exp(shifted)
    weights = weights / jnp.sum(weights, axis=-1, keepdims=True)
    weights_half = weights.astype(jnp.bfloat16)
    attended = jnp.einsum(
        "bhqk,bkhd->bqhd", weights_half, mine_values, preferred_element_type=jnp.float32
    )
    row_delta = jnp.sum(grad_in.astype(jnp.float32) * attended, axis=-1)
    grad_weights = jnp.einsum(
        "bqhd,bkhd->bhqk", grad_in, mine_values, preferred_element_type=jnp.float32
    )
    grad_scores = weights * (grad_weights - jnp.transpose(row_delta, (0, 2, 1))[..., None])
    grad_half = grad_scores.astype(jnp.bfloat16)
    grad_queries = (
        jnp.einsum("bhqk,bkhd->bqhd", grad_half, mine_keys, preferred_element_type=jnp.float32)
        * score_scale
    )
    grad_queries = grad_queries.reshape(tok_rows, local_width)
    grad_keys = (
        jnp.einsum("bhqk,bqhd->bkhd", grad_half, query_blocks, preferred_element_type=jnp.float32)
        * score_scale
    )
    grad_values = jnp.einsum(
        "bhqk,bqhd->bkhd", weights_half, grad_in, preferred_element_type=jnp.float32
    )
    grad_keys = grad_keys.reshape(slot_count, passage_len, local_width)
    grad_values = grad_values.reshape(slot_count, passage_len, local_width)
    empty_slots = jnp.zeros((st_size * slot_cap, passage_len, local_width), jnp.bfloat16)
    outgoing_keys = empty_slots.at[position].set(grad_keys.astype(jnp.bfloat16))
    outgoing_values = empty_slots.at[position].set(grad_values.astype(jnp.bfloat16))
    back_keys, back_values = (
        lax.all_to_all(outgoing_keys, "st", split_axis=0, concat_axis=0, tiled=True),
        lax.all_to_all(outgoing_values, "st", split_axis=0, concat_axis=0, tiled=True),
    )
    asked_flat = asked_ids.reshape(-1)
    owner_pick = (asked_flat[None, :] == jnp.arange(passages, dtype=jnp.int32)[:, None]).astype(
        jnp.bfloat16
    )
    passage_keys = jnp.dot(
        owner_pick,
        back_keys.reshape(st_size * slot_cap, passage_len * local_width),
        preferred_element_type=jnp.float32,
    )
    passage_values = jnp.dot(
        owner_pick,
        back_values.reshape(st_size * slot_cap, passage_len * local_width),
        preferred_element_type=jnp.float32,
    )
    passage_keys = passage_keys.astype(jnp.bfloat16).reshape(rows_dev, local_width)
    passage_values = passage_values.astype(jnp.bfloat16).reshape(rows_dev, local_width)
    weight_terms = lax.dot_general(
        normed, passage_values, (((0,), (0,)), ((), ())), preferred_element_type=jnp.float32
    )
    grad_w_value = lax.psum_scatter(weight_terms, "st", scatter_dimension=0, tiled=True)
    quarter = rows_dev // tp_size
    whole_key, whole_value = (
        lax.all_gather(w_key, "tp", axis=1, tiled=True),
        lax.all_gather(w_value, "tp", axis=1, tiled=True),
    )
    own_keys, own_values = (
        lax.all_to_all(passage_keys, "tp", split_axis=0, concat_axis=1, tiled=True),
        lax.all_to_all(passage_values, "tp", split_axis=0, concat_axis=1, tiled=True),
    )
    grad_normed = contract(own_keys, whole_key) + contract(own_values, whole_value)
    first_row = lax.axis_index("tp") * quarter
    own_rows = lax.dynamic_slice_in_dim(store_rows, first_row, quarter, 0)
    own_inverse = lax.dynamic_slice_in_dim(row_inverse, first_row, quarter, 0)
    unit_rows = own_rows * own_inverse
    grad_unit = grad_normed * store_gain
    grad_store = own_inverse * (
        grad_unit - unit_rows * jnp.mean(grad_unit * unit_rows, axis=-1, keepdims=True)
    )
    return (grad_queries, grad_store, grad_w_value)

FAR = 1e30
MESH = pl.DeviceIdType.MESH
NT = (((1,), (1,)), ((), ()))
TN = (((0,), (0,)), ((), ()))
CHUNK = 128


def place_of(index, n):
    odd = index % 2
    return (1 - odd) * (index // 2) + odd * (n - 1 - index // 2)


def index_at(place, n):
    place = (place + 2 * n) % n
    back = place // (n // 2)
    return (1 - back) * (2 * place) + back * (2 * (n - 1 - place) + 1)


def dot(left, right, dims=(((1,), (0,)), ((), ()))):
    return lax.dot_general(left, right, dims, preferred_element_type=jnp.float32)


def as_float(flag):
    return jnp.where(flag, jnp.float32(1.0), jnp.float32(0.0))


def rows_of_table(named, first, passages):
    total = named.shape[0]
    held = (named - first).astype(jnp.float32)
    inside = (held >= 0.0) & (held < passages)
    col = jnp.max(jnp.where(inside, held, -1.0), axis=1, keepdims=True)
    spot_col = lax.broadcasted_iota(jnp.int32, (128, 128), 0).astype(jnp.float32)
    spot_row = lax.broadcasted_iota(jnp.int32, (128, 128), 1).astype(jnp.float32)
    wide = jnp.broadcast_to(col, (total, 128))
    if total < 128:
        wide = jnp.concatenate([wide, jnp.full((128 - total, 128), 1000.0, jnp.float32)], axis=0)
    ids_row = wide.T
    key_col = wide * 128.0 + spot_col
    key_row = key_col.T
    rank_col = jnp.sum(as_float(key_row < key_col), axis=1, keepdims=True)
    rank_row = jnp.sum(as_float(key_col < key_row), axis=0, keepdims=True)
    order_row = jnp.sum(as_float(rank_col == spot_row) * spot_col, axis=0, keepdims=True)
    last_row = jnp.sum(as_float(wide <= spot_row), axis=0, keepdims=True) - 1.0
    has_row = jnp.max(as_float(wide == spot_row), axis=0, keepdims=True)
    rows = [ids_row[:1], rank_row, order_row, jnp.maximum(last_row, 0.0), has_row, jnp.zeros((3, 128), jnp.float32)]
    return jnp.concatenate(rows, axis=0).astype(jnp.int32)


IDS, RANK, ORDER, LAST, HAS = range(5)


def whole_kernel(n, tp, q_hbm, gate_hbm, cot_hbm, x_hbm, wk_hbm, wv_hbm, gain_ref, named_ref,
                 dq_ref, gs_ref, gw_ref,
                 q_all, g_all, i_all, gate_buf, cot_buf, x_buf, own_x, normed, whole, kt, vt,
                 tab_buf, tab, stats, got, joined, dq_sorted, tk, tv, pk, pv, pv_flip, own_kv,
                 dq_send, dq_recv, w_send, w_recv,
                 in_sem, x_sem, g_send, g_recv, i_send, i_recv, j_send, j_recv,
                 s_send, s_recv, ws_send, ws_recv, p_send, p_recv, t_send, t_recv, tab_sem):
    me, mine = lax.axis_index("st"), lax.axis_index("tp")
    place = place_of(me, n)
    right, left = index_at(place + 1, n), index_at(place - 1, n)
    hops = n // 2
    heads = len(q_all)
    total, block_len = q_all[0].shape[:2]
    blocks = total // n
    passages = kt[0].shape[0]
    rows_dev, features = normed.shape
    quarter = rows_dev // tp
    width = heads * HD
    feats = features // n
    scale = HD ** (-0.5)
    sibling = mine + 1 - 2 * (mine % 2)
    across = (mine + tp // 2) % tp
    half = blocks // 2

    barrier = pltpu.get_barrier_semaphore()
    for away in range(1, n):
        pl.semaphore_signal(barrier, inc=1, device_id={"st": (me + away) % n}, device_id_type=MESH)
    for away in range(1, tp):
        pl.semaphore_signal(barrier, inc=1, device_id={"tp": (mine + away) % tp}, device_id_type=MESH)

    def columns(owner, value):
        return pl.ds(pl.multiple_of(value * tp * width + owner * width, 128), width)

    loads = []
    for head in range(heads):
        loads.append(pltpu.make_async_copy(q_hbm.at[:, :, pl.ds(head * HD, HD)], q_all[head].at[pl.ds(me * blocks, blocks)], in_sem.at[head]))
    load_gate = pltpu.make_async_copy(gate_hbm, gate_buf, in_sem.at[heads])
    load_cot = pltpu.make_async_copy(cot_hbm, cot_buf, in_sem.at[heads + 1])
    load_w = [pltpu.make_async_copy(ref, whole.at[:, columns(mine, number)], in_sem.at[heads + 2 + number]) for number, ref in enumerate((wk_hbm, wv_hbm))]
    load_own = pltpu.make_async_copy(x_hbm.at[pl.ds(pl.multiple_of(mine * quarter, 16), quarter)], own_x, in_sem.at[heads + 4])

    def load_x(chunk):
        return pltpu.make_async_copy(x_hbm.at[pl.ds(chunk * CHUNK, CHUNK)], x_buf.at[chunk % 2], x_sem.at[chunk % 2])

    for copy in loads:
        copy.start()
    load_gate.start()
    load_cot.start()
    for copy in load_w:
        copy.start()
    load_x(0).start()
    load_own.start()

    sends = []

    def begin(copy):
        copy.start()
        sends.append(copy)

    def remote(src, dst, send_sem, recv_sem, **to):
        return pltpu.make_async_remote_copy(src_ref=src, dst_ref=dst, send_sem=send_sem, recv_sem=recv_sem, device_id=to, device_id_type=MESH)

    parts = ((0, 0), (0, 1), (1, 0), (1, 1))

    def gather_piece(head, side, step, part):
        number, which = parts[part]
        ref = (q_all, g_all)[number][head]
        origin = index_at(place - step, n) if side == 0 else index_at(place + step, n)
        at = ref.at[pl.ds(origin * blocks + which * half, half)]
        return remote(at, at, g_send.at[head, side, step, part], g_recv.at[head, side, step, part], st=right if side == 0 else left)

    def goes(side, step, part):
        return step < hops - 1 or parts[part][1] == side

    def ids_piece(away):
        return remote(named_ref, i_all.at[me], i_send.at[away], i_recv.at[away], st=(me + away) % n)

    def weight_piece(number, way):
        owner = mine if way < 2 else across
        at = whole.at[:, columns(owner, number)]
        return remote(at, at, t_send.at[number, way], t_recv.at[number, way], tp=across if way == 1 else sibling)

    def make_grad_in():
        load_gate.wait()
        load_cot.wait()

        @pl.loop(0, blocks)
        def _(block):
            for head in range(heads):
                cols = pl.ds(head * HD, HD)
                opened = jax.nn.sigmoid(gate_buf[block, :, cols].astype(jnp.float32))
                g_all[head][me * blocks + block] = (opened * cot_buf[block, :, cols].astype(jnp.float32)).astype(jnp.bfloat16)

    def project(chunk):
        if (chunk + 1) * CHUNK < rows_dev:
            load_x(chunk + 1).start()
        load_x(chunk).wait()
        rows = pl.ds(chunk * CHUNK, CHUNK)
        wide = x_buf[chunk % 2].astype(jnp.float32)
        ready = (wide * row_scale(wide) * gain_ref[...]).astype(jnp.bfloat16)
        normed[rows] = ready
        per = CHUNK // PLEN
        for number, table in enumerate((kt, vt)):
            out = dot(ready, whole[:, columns(mine, number)]).astype(jnp.bfloat16)
            for head in range(heads):
                table[head][pl.ds(chunk * per, per)] = out[:, head * HD:(head + 1) * HD].reshape(per, PLEN, HD)

    def make_table():
        for away in range(1, n):
            ids_piece(away).wait_recv()
        tab_buf[...] = rows_of_table(i_all[...].reshape(total, 128), me * passages, passages)
        copy = pltpu.make_async_copy(tab_buf, tab, tab_sem.at[0])
        copy.start()
        copy.wait()

    def make_stats(head, origin):
        for first in range(0, blocks, 4):
            count = min(4, blocks - first)
            spots = [origin * blocks + first + lane for lane in range(count)]
            ids = [jnp.minimum(tab[IDS, spot], passages - 1) for spot in spots]
            scores = [dot(kt[head][jnp.maximum(one, 0)], q_all[head][spot], NT) * scale for one, spot in zip(ids, spots)]
            grads = [dot(vt[head][jnp.maximum(one, 0)], g_all[head][spot], NT) for one, spot in zip(ids, spots)]
            tops = [jnp.max(one, axis=0, keepdims=True) for one in scores]
            raised = [jnp.exp(one - top) for one, top in zip(scores, tops)]
            totals = [jnp.sum(one, axis=0, keepdims=True) for one in raised]
            means = [jnp.sum(one * two, axis=0, keepdims=True) / three for one, two, three in zip(raised, grads, totals)]
            for lane in range(count):
                dead = jnp.minimum(ids[lane], 0).astype(jnp.float32) * FAR
                stats[head][origin, 0, pl.ds(first + lane, 1)] = tops[lane] + jnp.log(totals[lane]) + dead
                stats[head][origin, 1, pl.ds(first + lane, 1)] = means[lane]

    def join_piece(head, phase, away):
        peer = (me + away) % n
        at = joined[head].at[pl.ds(me * blocks, blocks)]
        return remote(
            stats[head].at[peer] if phase == 0 else at,
            got[head].at[me] if phase == 0 else at,
            j_send.at[head, phase, away], j_recv.at[head, phase, away], st=peer)

    def join_first(head):
        for away in range(1, n):
            begin(join_piece(head, 0, away))
        got[head][me] = stats[head][me]

    def join_second(head):
        for away in range(1, n):
            join_piece(head, 0, away).wait_recv()
        logs = [got[head][owner, 0] for owner in range(n)]
        top = functools.reduce(jnp.maximum, logs)
        shares = [jnp.exp(one - top) for one in logs]
        whole_sum = sum(shares)
        final = top + jnp.log(whole_sum)
        mean = sum(share * got[head][owner, 1] for owner, share in enumerate(shares)) / whole_sum
        for block in range(blocks):
            joined[head][me * blocks + block, 0:1] = final[block:block + 1]
            joined[head][me * blocks + block, 1:2] = mean[block:block + 1]
        for away in range(1, n):
            begin(join_piece(head, 1, away))

    def join_last(head):
        for away in range(1, n):
            join_piece(head, 1, away).wait_recv()

    lanes = 4

    def make_grads(head, begin_turn, end_turn, carry):
        def turn_body(turn, carry):
            acc_k, acc_v, past = carry
            spots = [jnp.clip(tab[ORDER, turn * lanes + lane], 0, total - 1) for lane in range(lanes)]
            ids = [jnp.minimum(tab[IDS, spot], passages - 1) for spot in spots]
            keys = [kt[head][jnp.maximum(one, 0)] for one in ids]
            queries = [q_all[head][spot] for spot in spots]
            givens = [g_all[head][spot] for spot in spots]
            scores = [dot(key, query, NT) * scale for key, query in zip(keys, queries)]
            grads = [dot(vt[head][jnp.maximum(one, 0)], given, NT) for one, given in zip(ids, givens)]
            weights, halves = [], []
            for one, spot, score, grad in zip(ids, spots, scores, grads):
                logs = joined[head][spot, 0:1] - jnp.minimum(one, 0).astype(jnp.float32) * FAR
                weight = jnp.exp(score - logs)
                halves.append((weight * (grad - joined[head][spot, 1:2])).astype(jnp.bfloat16))
                weights.append(weight.astype(jnp.bfloat16))
            term_k = [dot(one, query) for one, query in zip(halves, queries)]
            term_v = [dot(one, given) for one, given in zip(weights, givens)]
            steps = [dot(one, key, TN) for one, key in zip(halves, keys)]
            for lane in range(lanes):
                keep = as_float(ids[lane] == past)
                past = ids[lane]
                acc_k = acc_k * keep + term_k[lane]
                acc_v = acc_v * keep + term_v[lane]
                at = turn * lanes + lane
                tk[head][at] = (acc_k * scale).astype(jnp.bfloat16)
                tv[head][at] = acc_v.astype(jnp.bfloat16)
                dq_sorted[head][at] = (steps[lane] * scale).astype(jnp.bfloat16)
            return acc_k, acc_v, past

        return lax.fori_loop(begin_turn, end_turn, turn_body, carry)

    blank = (jnp.zeros((PLEN, HD), jnp.float32), jnp.zeros((PLEN, HD), jnp.float32), jnp.int32(-2))
    turns = total // lanes

    def pick(head):
        @pl.loop(0, passages)
        def _(passage):
            last = jnp.clip(tab[LAST, passage], 0, total - 1)
            has = tab[HAS, passage].astype(jnp.float32)
            rows = pl.ds(pl.multiple_of(passage * PLEN, PLEN), PLEN)
            pk[head][rows] = (tk[head][last].astype(jnp.float32) * has).astype(jnp.bfloat16)
            pv[head][rows] = (tv[head][last].astype(jnp.float32) * has).astype(jnp.bfloat16)

    def own_columns(owner, head, number):
        return pl.ds(pl.multiple_of(number * tp * width + owner * width + head * HD, 128), HD)

    def passage_piece(head, number, away):
        peer = (mine + away) % tp
        rows = pl.ds(pl.multiple_of(peer * quarter, 16), quarter)
        return remote((pk, pv)[number][head].at[rows], own_kv.at[:, own_columns(mine, head, number)],
                      p_send.at[head, number, away], p_recv.at[head, number, away], tp=peer)

    def share(head):
        for number in range(2):
            for away in range(1, tp):
                begin(passage_piece(head, number, away))
            rows = pl.ds(pl.multiple_of(mine * quarter, 16), quarter)
            own_kv[:, own_columns(mine, head, number)] = (pk, pv)[number][head][rows]

    dq_parts = ((0, 0), (half, 1), (half // 2, 0), (half + half // 2, 1))
    dq_count = half // 2

    def used(side, step, part):
        return step > 0 or dq_parts[part][1] == side

    def dq_piece(head, side, step, part):
        at = pl.ds(dq_parts[part][0], dq_count)
        return remote(dq_send[head].at[side, step, at], dq_recv[head].at[side, step, at],
                      s_send.at[head, side, step, part], s_recv.at[head, side, step, part], st=right if side == 0 else left)

    def dest_of(side, step):
        distance = hops - step
        return index_at(place + distance, n) if side == 0 else index_at(place - distance, n)

    def dq_step(head, step, part):
        for side in range(2):
            if not used(side, step, part):
                continue
            dest = dest_of(side, step)
            arrived = step > 0 and used(side, step - 1, part)
            if arrived:
                dq_piece(head, side, step - 1, part).wait_recv()
            for lane in range(dq_count):
                block = dq_parts[part][0] + lane
                value = dq_sorted[head][jnp.clip(tab[RANK, dest * blocks + block], 0, total - 1)]
                if arrived:
                    value = (value.astype(jnp.float32) + dq_recv[head][side, step - 1, block].astype(jnp.float32)).astype(jnp.bfloat16)
                dq_send[head][side, step, block] = value
            begin(dq_piece(head, side, step, part))

    def dq_end(head, part):
        for side in range(2):
            dq_piece(head, side, hops - 1, part).wait_recv()
        for lane in range(dq_count):
            block = dq_parts[part][0] + lane
            value = dq_sorted[head][jnp.clip(tab[RANK, me * blocks + block], 0, total - 1)].astype(jnp.float32)
            for side in range(2):
                value = value + dq_recv[head][side, hops - 1, block].astype(jnp.float32)
            dq_ref[pl.ds(block * block_len, block_len), pl.ds(head * HD, HD)] = value

    def w_piece(side, step, part):
        at = pl.ds(part * HD, HD)
        return remote(w_send.at[side, step, at], w_recv.at[side, step, at],
                      ws_send.at[side, step, part], ws_recv.at[side, step, part], st=right if side == 0 else left)

    def w_term(dest, part):
        return dot(pv_flip[pl.ds(part * HD, HD)], normed[:, pl.ds(pl.multiple_of(dest * feats, 128), feats)])

    def w_used(side, step, part):
        return step > 0 or part % 2 == side

    def w_step(step, part):
        for side in range(2):
            if not w_used(side, step, part):
                continue
            value = w_term(dest_of(side, step), part)
            at = pl.ds(part * HD, HD)
            if step > 0 and w_used(side, step - 1, part):
                w_piece(side, step - 1, part).wait_recv()
                value = value + w_recv[side, step - 1, at].astype(jnp.float32)
            w_send[side, step, at] = value.astype(jnp.bfloat16)
            begin(w_piece(side, step, part))

    def w_end(part):
        at = pl.ds(part * HD, HD)
        value = w_term(me, part)
        for side in range(2):
            w_piece(side, hops - 1, part).wait_recv()
            value = value + w_recv[side, hops - 1, at].astype(jnp.float32)
        gw_ref[:, pl.ds(part * HD, HD)] = value.T

    def flip():
        for head in range(heads):
            for first in range(0, rows_dev, 256):
                pv_flip[pl.ds(head * HD, HD), pl.ds(first, 256)] = pv[head][pl.ds(first, 256)].astype(jnp.float32).T.astype(jnp.bfloat16)

    slab = 256

    def store_slab(number):
        cols = pl.ds(number * slab, slab)
        gs_ref[:, cols] = dot(own_kv[...], whole[cols], NT) * gain_ref[:, cols]

    def store_end(first, count):
        rows = pl.ds(first, count)
        wide = own_x[rows].astype(jnp.float32)
        inverse = row_scale(wide)
        unit = wide * inverse
        value = gs_ref[rows]
        gs_ref[rows] = inverse * (value - unit * jnp.mean(value * unit, axis=-1, keepdims=True))

    for copy in loads:
        copy.wait()
    pl.semaphore_wait(barrier, n - 1 + tp - 1)
    for away in range(1, n):
        begin(ids_piece(away))
    for part in range(2):
        for side in range(2):
            begin(gather_piece(0, side, 0, part))
    for copy in load_w:
        copy.wait()
    for number in range(2):
        begin(weight_piece(number, 1))
        begin(weight_piece(number, 0))
    i_all[me] = named_ref[...]
    make_grad_in()
    for part in range(2, 4):
        for side in range(2):
            begin(gather_piece(0, side, 0, part))

    tasks = [functools.partial(project, chunk) for chunk in range(rows_dev // CHUNK)]
    tasks.append(make_table)
    tasks.append(functools.partial(make_stats, 0, me))

    def fill(count=1):
        for _ in range(count):
            if tasks:
                tasks.pop(0)()

    def arrived_at(head, step):
        return [functools.partial(make_stats, head, index_at(place - step, n)), functools.partial(make_stats, head, index_at(place + step, n))]

    state = {0: blank, 1: blank}

    def grads_task(head, first, last):
        def run():
            state[head] = make_grads(head, first, last, state[head])
        return run

    def grad_tasks(head, pieces):
        edges = [turns * piece // pieces for piece in range(pieces + 1)]
        return [grads_task(head, edges[piece], edges[piece + 1]) for piece in range(pieces)]

    def gather_step(head, step):
        for part in range(4):
            for side in range(2):
                if goes(side, step, part):
                    if step > 0:
                        gather_piece(head, side, step - 1, part).wait_recv()
                    begin(gather_piece(head, side, step, part))
            fill()

    def gather_rest(head, first):
        if first:
            for part in range(4):
                for side in range(2):
                    if not goes(side, hops - 1, part):
                        gather_piece(head, side, hops - 2, part).wait_recv()
        else:
            for part in range(4):
                gather_piece(head, parts[part][1], hops - 1, part).wait_recv()

    for step in range(1, hops):
        gather_step(0, step)
        if step > 1:
            tasks.extend(arrived_at(0, step - 1))
    for part in range(4):
        for side in range(2):
            begin(gather_piece(1, side, 0, part))
        fill()
    gather_rest(0, True)
    tasks.extend(arrived_at(0, hops - 1))
    fill(len(tasks))
    gather_rest(0, False)
    make_stats(0, index_at(place + hops, n))
    join_first(0)
    tasks.append(functools.partial(make_stats, 1, me))
    gather_step(1, 1)
    join_second(0)
    for number in range(2):
        weight_piece(number, 1).wait_recv()
        begin(weight_piece(number, 2))
    if hops > 2:
        gather_step(1, 2)
        tasks.extend(arrived_at(1, 1))
    join_last(0)
    tasks[0:0] = grad_tasks(0, 4)
    for step in range(max(3, hops - 1), hops):
        gather_step(1, step)
        tasks.extend(arrived_at(1, step - 1))
    tasks.append(functools.partial(pick, 0))
    fill(len(tasks))
    share(0)
    for part in range(4):
        dq_step(0, 0, part)
    gather_rest(1, True)
    for task in arrived_at(1, hops - 1):
        task()
    gather_rest(1, False)
    make_stats(1, index_at(place + hops, n))
    join_first(1)
    for part in range(4):
        dq_step(0, 1, part)
    join_second(1)
    for part in range(4):
        dq_step(0, 2 % hops, part) if hops > 2 else None
    join_last(1)
    tasks.extend(grad_tasks(1, 4))
    for step in range(3, hops):
        for part in range(4):
            dq_step(0, step, part)
            fill()
    fill(len(tasks))
    for part in range(4):
        dq_step(1, 0, part)
    pick(1)
    share(1)
    flip()
    for part in range(heads):
        w_step(0, part)
    for part in range(4):
        dq_end(0, part)
    for number in range(2):
        for way in (0, 2):
            weight_piece(number, way).wait_recv()
    for head in range(heads):
        for number in range(2):
            for away in range(1, tp):
                passage_piece(head, number, away).wait_recv()
    tasks.extend([functools.partial(store_slab, number) for number in range(features // slab)])
    load_own.wait()
    ending = 64
    tasks.extend([functools.partial(store_end, first, min(ending, quarter - first)) for first in range(0, quarter, ending)])
    for step in range(1, hops):
        for part in range(4):
            dq_step(1, step, part)
            fill()
        for part in range(heads):
            w_step(step, part)
    fill(len(tasks))
    for part in range(4):
        dq_end(1, part)
    for part in range(heads):
        w_end(part)
    for copy in sends:
        copy.wait_send()


def query_plan(queries, gate_pre, cotangent, store, store_gain, w_key, w_value, owners, slots):
    n = lax.axis_size("st")
    tp = lax.axis_size("tp")
    blocks, per_block = owners.shape
    tok_rows, width = queries.shape
    heads = width // HD
    block_len = tok_rows // blocks
    rows_dev, features = store.shape
    passages = rows_dev // PLEN
    quarter = rows_dev // tp
    total = n * blocks
    hops = n // 2
    feats = features // n
    named = jnp.pad(owners * passages + slots, ((0, 0), (0, 128 - per_block)), constant_values=-1)
    blocked = [one.reshape(blocks, block_len, width) for one in (queries, gate_pre, cotangent)]
    vmem = pl.BlockSpec(memory_space=pltpu.VMEM)
    anywhere = pl.BlockSpec(memory_space=pl.ANY)
    half, wide = jnp.bfloat16, jnp.float32
    dma = pltpu.SemaphoreType.DMA

    def per_head(shape, kind):
        return [pltpu.VMEM(shape, kind) for _ in range(heads)]

    return pl.pallas_call(
        functools.partial(whole_kernel, n, tp),
        out_shape=(
            jax.ShapeDtypeStruct((tok_rows, width), wide),
            jax.ShapeDtypeStruct((quarter, features), wide),
            jax.ShapeDtypeStruct((feats, width), wide),
        ),
        in_specs=[anywhere] * 6 + [vmem] * 2,
        out_specs=(vmem,) * 3,
        scratch_shapes=[
            per_head((total, block_len, HD), half),
            per_head((total, block_len, HD), half),
            pltpu.VMEM((n, blocks, 128), jnp.int32),
            pltpu.VMEM((blocks, block_len, width), half),
            pltpu.VMEM((blocks, block_len, width), half),
            pltpu.VMEM((2, CHUNK, features), half),
            pltpu.VMEM((quarter, features), half),
            pltpu.VMEM((rows_dev, features), half),
            pltpu.VMEM((features, 2 * tp * width), half),
            per_head((passages, PLEN, HD), half),
            per_head((passages, PLEN, HD), half),
            pltpu.VMEM((8, 128), jnp.int32),
            pltpu.SMEM((8, 128), jnp.int32),
            per_head((n + 1, 2, blocks, block_len), wide),
            per_head((n, 2, blocks, block_len), wide),
            per_head((total + 4, 2, block_len), wide),
            per_head((total, block_len, HD), half),
            per_head((total, PLEN, HD), half),
            per_head((total, PLEN, HD), half),
            per_head((rows_dev, HD), half),
            per_head((rows_dev, HD), half),
            pltpu.VMEM((width, rows_dev), half),
            pltpu.VMEM((quarter, 2 * tp * width), half),
            per_head((2, hops, blocks, block_len, HD), half),
            per_head((2, hops, blocks, block_len, HD), half),
            pltpu.VMEM((2, hops, width, feats), half),
            pltpu.VMEM((2, hops, width, feats), half),
            dma((heads + 5,)),
            dma((2,)),
            dma((heads, 2, hops, 4)),
            dma((heads, 2, hops, 4)),
            dma((n,)),
            dma((n,)),
            dma((heads, 2, n)),
            dma((heads, 2, n)),
            dma((heads, 2, hops, 4)),
            dma((heads, 2, hops, 4)),
            dma((2, hops, heads)),
            dma((2, hops, heads)),
            dma((heads, 2, tp)),
            dma((heads, 2, tp)),
            dma((2, 3)),
            dma((2, 3)),
            dma((1,)),
        ],
        cost_estimate=pl.CostEstimate(flops=2 * 10**10, bytes_accessed=3 * 10**7, transcendentals=0),
        compiler_params=pltpu.CompilerParams(collective_id=0, has_side_effects=True, vmem_limit_bytes=60 << 20),
        name="whole",
    )(*blocked, store, w_key, w_value, store_gain[None], named)


def fits(queries, store, owners):
    n, tp = lax.axis_size("st"), lax.axis_size("tp")
    blocks = owners.shape[0]
    block_len = queries.shape[0] // blocks
    slot_cap = (2 * owners.size + n - 1) // n
    return (
        n % 2 == 0 and n >= 8 and tp == 4 and blocks == 8 and n * blocks <= 128
        and block_len == 128 and queries.shape[1] == 2 * HD
        and store.shape[0] % (tp * CHUNK // 2) == 0 and store.shape[0] % 256 == 0
        and store.shape[0] // PLEN <= 128 and store.shape[1] % (256 * n) == 0
        and 8 * slot_cap * PLEN >= 3 * queries.shape[0]
    )


def local(*arrays):
    if fits(arrays[0], arrays[3], arrays[7]):
        return query_plan(*arrays)
    return passage_plan(*arrays)


def solution(mesh):
    placed = (
        P("st", "tp"),
        P("st", "tp"),
        P("st", "tp"),
        P("st", None),
        P(),
        P(None, "tp"),
        P(None, "tp"),
        P("st", None),
        P("st", None),
    )
    return jax.shard_map(
        local,
        mesh=mesh,
        in_specs=placed,
        out_specs=(P("st", "tp"), P(("st", "tp"), None), P("st", "tp")),
        check_vma=False,
    )
```

time: 248 us -> 162 us (0.65)
  Pallas kernels: 186 us -> 152 us
  matrix products: 15.7 us -> 0 us
  between operations: 14.9 us -> 0.64 us
  local copies, waits for them, and re-layouts: 19.1 us -> 8.66 us
  other arithmetic: 7.64 us -> 0.01 us
    pallas_call x5 -> x1, Pallas kernels: 186 us -> 152 us  [query_plan(): pl.pallas_call(functools.partial(whole_kernel, n, tp), out_shape=(jax.Sha...]
    dot_general x3 -> x0, matrix products: 15.7 us -> none  [the longest x2 10.6 us: contract(): lax.dot_general(left, right, (((1,), (1,)), ((), ())), preferred_element_...]
    unnamed x30 -> x7, local copies, waits for them, and re-layouts: 19.1 us -> 8.06 us
    mul x1 -> x0, other arithmetic: 3.33 us -> none  [query_plan(): own_inverse * (grad_unit - unit_rows * jnp.mean(grad_unit * unit_rows, ax...]
  transfers between devices with their start and end apart: 2 -> 0, of which waited for: 0 -> 0; matrix products, arithmetic and copies ran while one was open for 7% -> 0% of each run, Pallas kernels for 76% -> 0%
where the time goes in v1:
time: 162 us; the launch traced here: 161 us
  Pallas kernels  152 us (94%)
  local copies, waits for them, and re-layouts  8.66 us (5%)
    pallas_call x1, Pallas kernels, query_plan(): pl.pallas_call(functools.partial(whole_kernel, n, tp), out_shape=(jax.Sha...  152 us
    unnamed x7, local copies, waits for them, and re-layouts  8.06 us

profile of v1, /device:TPU:0, one launch (start us, length us, event | category | flops | bytes accessed | tf_op | source)
XLA Modules:
  0.0 161.5 jit_solution(6408519949054770967)
XLA Ops:
  0.6 0.8 copy.12
  1.4 0.8 copy.13
  2.1 0.6 pad.4.named_ref
  2.7 152.2 %whole.1 = (f32[1024,256]{1,0:T(8,128)}, f32[320,2048]{1,0:T(8,128)}, f32[256,256]{1,0:T(8,128)}) custom-call(bf16[8,128,256]{2,1,0:T(8,128)(2,1)} %bitcast.4, bf16[8,128,256]{2,1,0:T(8,128)(2,1)} %bitcast.5, bf16[8,128,256]{2,1,0:T(8,128)(2,1)} %bitcast.6, bf16[1280,2048]{1,0:T(8,128)(2,1)} %x_hbm.1, bf16[2048,256]{1,0:T(8,128)(2,1)} %wk_hbm.1, ...), custom_call_target="tpu_custom_call" | custom-call | flops 20000000000 | bytes 30000000 | tf_op jit(solution)/shard_map/whole/pallas_call | solution.py:696
  154.9 2.3 %copy.17 = f32[1024,256]{1,0:T(8,128)} copy(f32[1024,256]{1,0:T(8,128)} %get-tuple-element.6) | data formatting | bytes 2097152
  157.2 0.0 copy-start
  157.2 3.6 %copy.18 = f32[320,2048]{1,0:T(8,128)} copy(f32[320,2048]{1,0:T(8,128)} %get-tuple-element.7) | data formatting | bytes 5242880
  160.8 0.0 copy-done
  160.8 0.7 copy.19
  (1 shorter events, 0.0 us)
Async XLA Ops:
  157.2 3.6 %copy-start = (f32[256,256]{1,0:T(8,128)S(1)}, f32[256,256]{1,0:T(8,128)}, u32[]{:S(2)}) copy-start(f32[256,256]{1,0:T(8,128)} %get-tuple-element.8) | copy-start | bytes 786436

commit v2 on v1

--- a/solution.py
+++ b/solution.py
@@ -161,6 +161,7 @@
 NT = (((1,), (1,)), ((), ()))
 TN = (((0,), (0,)), ((), ()))
 CHUNK = 128
+VMEM_LIMIT = 45 << 20
 
 
 def place_of(index, n):
@@ -207,9 +208,9 @@
 IDS, RANK, ORDER, LAST, HAS = range(5)
 
 
-def whole_kernel(n, tp, q_hbm, gate_hbm, cot_hbm, x_hbm, wk_hbm, wv_hbm, gain_ref, named_ref,
+def whole_kernel(n, tp, q_hbm, gate_hbm, cot_hbm, x_hbm, wk_hbm, wv_hbm, gain_hbm, owners_hbm, slots_hbm,
                  dq_ref, gs_ref, gw_ref,
-                 q_all, g_all, i_all, gate_buf, cot_buf, x_buf, own_x, normed, whole, kt, vt,
+                 gain_ref, owners_buf, slots_buf, flat, named_ref, q_all, g_all, i_all, gate_buf, cot_buf, x_buf, own_x, normed, whole, kt, vt,
                  tab_buf, tab, stats, got, joined, dq_sorted, tk, tv, pk, pv, pv_flip, own_kv,
                  dq_send, dq_recv, w_send, w_recv,
                  in_sem, x_sem, g_send, g_recv, i_send, i_recv, j_send, j_recv,
@@ -246,19 +247,14 @@
     load_gate = pltpu.make_async_copy(gate_hbm, gate_buf, in_sem.at[heads])
     load_cot = pltpu.make_async_copy(cot_hbm, cot_buf, in_sem.at[heads + 1])
     load_w = [pltpu.make_async_copy(ref, whole.at[:, columns(mine, number)], in_sem.at[heads + 2 + number]) for number, ref in enumerate((wk_hbm, wv_hbm))]
+    load_small = [pltpu.make_async_copy(src, dst, in_sem.at[heads + 5 + number]) for number, (src, dst) in enumerate(((owners_hbm, owners_buf), (slots_hbm, slots_buf), (gain_hbm, gain_ref)))]
     load_own = pltpu.make_async_copy(x_hbm.at[pl.ds(pl.multiple_of(mine * quarter, 16), quarter)], own_x, in_sem.at[heads + 4])
 
     def load_x(chunk):
         return pltpu.make_async_copy(x_hbm.at[pl.ds(chunk * CHUNK, CHUNK)], x_buf.at[chunk % 2], x_sem.at[chunk % 2])
 
-    for copy in loads:
+    for copy in load_small[:2] + loads + [load_gate, load_cot] + load_w + load_small[2:] + [load_x(0), load_own]:
         copy.start()
-    load_gate.start()
-    load_cot.start()
-    for copy in load_w:
-        copy.start()
-    load_x(0).start()
-    load_own.start()
 
     sends = []
 
@@ -397,8 +393,8 @@
                 acc_k = acc_k * keep + term_k[lane]
                 acc_v = acc_v * keep + term_v[lane]
                 at = turn * lanes + lane
-                tk[head][at] = (acc_k * scale).astype(jnp.bfloat16)
-                tv[head][at] = acc_v.astype(jnp.bfloat16)
+                tk[at] = (acc_k * scale).astype(jnp.bfloat16)
+                tv[at] = acc_v.astype(jnp.bfloat16)
                 dq_sorted[head][at] = (steps[lane] * scale).astype(jnp.bfloat16)
             return acc_k, acc_v, past
 
@@ -413,8 +409,8 @@
             last = jnp.clip(tab[LAST, passage], 0, total - 1)
             has = tab[HAS, passage].astype(jnp.float32)
             rows = pl.ds(pl.multiple_of(passage * PLEN, PLEN), PLEN)
-            pk[head][rows] = (tk[head][last].astype(jnp.float32) * has).astype(jnp.bfloat16)
-            pv[head][rows] = (tv[head][last].astype(jnp.float32) * has).astype(jnp.bfloat16)
+            pk[head][rows] = (tk[last].astype(jnp.float32) * has).astype(jnp.bfloat16)
+            pv[head][rows] = (tv[last].astype(jnp.float32) * has).astype(jnp.bfloat16)
 
     def own_columns(owner, head, number):
         return pl.ds(pl.multiple_of(number * tp * width + owner * width + head * HD, 128), HD)
@@ -440,7 +436,8 @@
 
     def dq_piece(head, side, step, part):
         at = pl.ds(dq_parts[part][0], dq_count)
-        return remote(dq_send[head].at[side, step, at], dq_recv[head].at[side, step, at],
+        src = dq_recv[head].at[side, step - 1, at] if step > 0 else dq_send[head].at[at]
+        return remote(src, dq_recv[head].at[side, step, at],
                       s_send.at[head, side, step, part], s_recv.at[head, side, step, part], st=right if side == 0 else left)
 
     def dest_of(side, step):
@@ -460,7 +457,10 @@
                 value = dq_sorted[head][jnp.clip(tab[RANK, dest * blocks + block], 0, total - 1)]
                 if arrived:
                     value = (value.astype(jnp.float32) + dq_recv[head][side, step - 1, block].astype(jnp.float32)).astype(jnp.bfloat16)
-                dq_send[head][side, step, block] = value
+                if step > 0:
+                    dq_recv[head][side, step - 1, block] = value
+                else:
+                    dq_send[head][block] = value
             begin(dq_piece(head, side, step, part))
 
     def dq_end(head, part):
@@ -474,12 +474,12 @@
             dq_ref[pl.ds(block * block_len, block_len), pl.ds(head * HD, HD)] = value
 
     def w_piece(side, step, part):
-        at = pl.ds(part * HD, HD)
-        return remote(w_send.at[side, step, at], w_recv.at[side, step, at],
+        src = w_recv.at[side, step - 1, part] if step > 0 else w_send.at[part]
+        return remote(src, w_recv.at[side, step, part],
                       ws_send.at[side, step, part], ws_recv.at[side, step, part], st=right if side == 0 else left)
 
     def w_term(dest, part):
-        return dot(pv_flip[pl.ds(part * HD, HD)], normed[:, pl.ds(pl.multiple_of(dest * feats, 128), feats)])
+        return dot(pv_flip[part], normed[:, pl.ds(pl.multiple_of(dest * feats, 128), feats)])
 
     def w_used(side, step, part):
         return step > 0 or part % 2 == side
@@ -489,25 +489,25 @@
             if not w_used(side, step, part):
                 continue
             value = w_term(dest_of(side, step), part)
-            at = pl.ds(part * HD, HD)
             if step > 0 and w_used(side, step - 1, part):
                 w_piece(side, step - 1, part).wait_recv()
-                value = value + w_recv[side, step - 1, at].astype(jnp.float32)
-            w_send[side, step, at] = value.astype(jnp.bfloat16)
+                value = value + w_recv[side, step - 1, part].astype(jnp.float32)
+            if step > 0:
+                w_recv[side, step - 1, part] = value.astype(jnp.bfloat16)
+            else:
+                w_send[part] = value.astype(jnp.bfloat16)
             begin(w_piece(side, step, part))
 
     def w_end(part):
-        at = pl.ds(part * HD, HD)
         value = w_term(me, part)
         for side in range(2):
             w_piece(side, hops - 1, part).wait_recv()
-            value = value + w_recv[side, hops - 1, at].astype(jnp.float32)
+            value = value + w_recv[side, hops - 1, part].astype(jnp.float32)
         gw_ref[:, pl.ds(part * HD, HD)] = value.T
 
-    def flip():
-        for head in range(heads):
-            for first in range(0, rows_dev, 256):
-                pv_flip[pl.ds(head * HD, HD), pl.ds(first, 256)] = pv[head][pl.ds(first, 256)].astype(jnp.float32).T.astype(jnp.bfloat16)
+    def flip(head):
+        for first in range(0, rows_dev, 256):
+            pv_flip[head, :, pl.ds(first, 256)] = pv[head][pl.ds(first, 256)].astype(jnp.float32).T.astype(jnp.bfloat16)
 
     slab = 256
 
@@ -523,36 +523,51 @@
         value = gs_ref[rows]
         gs_ref[rows] = inverse * (value - unit * jnp.mean(value * unit, axis=-1, keepdims=True))
 
-    for copy in loads:
+    for copy in load_small[:2]:
         copy.wait()
+    per_block = owners_buf.shape[0]
+    flat[...] = jnp.full(flat.shape, -1.0, jnp.float32)
+    flat[pl.ds(0, per_block), pl.ds(0, blocks)] = (owners_buf[...] * passages + slots_buf[...]).astype(jnp.float32)
+    named_ref[...] = jnp.full(named_ref.shape, -1, jnp.int32)
+    named_ref[:, pl.ds(0, 8)] = flat[...].T[:blocks].astype(jnp.int32)
+    loads[0].wait()
     pl.semaphore_wait(barrier, n - 1 + tp - 1)
-    for away in range(1, n):
-        begin(ids_piece(away))
     for part in range(2):
         for side in range(2):
             begin(gather_piece(0, side, 0, part))
+    make_grad_in()
+    for part in range(2, 4):
+        for side in range(2):
+            begin(gather_piece(0, side, 0, part))
+    for away in range(1, n):
+        begin(ids_piece(away))
+    i_all[me] = named_ref[...]
     for copy in load_w:
         copy.wait()
     for number in range(2):
         begin(weight_piece(number, 1))
         begin(weight_piece(number, 0))
-    i_all[me] = named_ref[...]
-    make_grad_in()
-    for part in range(2, 4):
-        for side in range(2):
-            begin(gather_piece(0, side, 0, part))
+    load_small[2].wait()
+    for copy in loads[1:]:
+        copy.wait()
 
     tasks = [functools.partial(project, chunk) for chunk in range(rows_dev // CHUNK)]
     tasks.append(make_table)
     tasks.append(functools.partial(make_stats, 0, me))
+
+    def idle():
+        pass
 
     def fill(count=1):
         for _ in range(count):
             if tasks:
                 tasks.pop(0)()
 
-    def arrived_at(head, step):
-        return [functools.partial(make_stats, head, index_at(place - step, n)), functools.partial(make_stats, head, index_at(place + step, n))]
+    def both(head, step):
+        def run():
+            make_stats(head, index_at(place - step, n))
+            make_stats(head, index_at(place + step, n))
+        return run
 
     state = {0: blank, 1: blank}
 
@@ -584,66 +599,70 @@
             for part in range(4):
                 gather_piece(head, parts[part][1], hops - 1, part).wait_recv()
 
+    def forward_weights():
+        for number in range(2):
+            weight_piece(number, 1).wait_recv()
+            begin(weight_piece(number, 2))
+
     for step in range(1, hops):
         gather_step(0, step)
-        if step > 1:
-            tasks.extend(arrived_at(0, step - 1))
+        if step < hops - 1:
+            tasks.append(both(0, step))
     for part in range(4):
         for side in range(2):
             begin(gather_piece(1, side, 0, part))
         fill()
     gather_rest(0, True)
-    tasks.extend(arrived_at(0, hops - 1))
+    tasks.append(both(0, hops - 1))
     fill(len(tasks))
     gather_rest(0, False)
     make_stats(0, index_at(place + hops, n))
     join_first(0)
-    tasks.append(functools.partial(make_stats, 1, me))
+    tasks.extend([functools.partial(make_stats, 1, me), idle, functools.partial(join_second, 0), forward_weights])
     gather_step(1, 1)
-    join_second(0)
-    for number in range(2):
-        weight_piece(number, 1).wait_recv()
-        begin(weight_piece(number, 2))
-    if hops > 2:
-        gather_step(1, 2)
-        tasks.extend(arrived_at(1, 1))
-    join_last(0)
-    tasks[0:0] = grad_tasks(0, 4)
-    for step in range(max(3, hops - 1), hops):
+    tasks.extend([both(1, 1), idle, idle, functools.partial(join_last, 0)])
+    gather_step(1, 2)
+    tasks.extend(grad_tasks(0, 4))
+    tasks.extend([functools.partial(pick, 0), functools.partial(share, 0), functools.partial(flip, 0)])
+    for step in range(3, hops):
         gather_step(1, step)
-        tasks.extend(arrived_at(1, step - 1))
-    tasks.append(functools.partial(pick, 0))
     fill(len(tasks))
-    share(0)
     for part in range(4):
         dq_step(0, 0, part)
+    for step in range(2, hops - 1):
+        both(1, step)()
     gather_rest(1, True)
-    for task in arrived_at(1, hops - 1):
-        task()
+    both(1, hops - 1)()
     gather_rest(1, False)
     make_stats(1, index_at(place + hops, n))
     join_first(1)
+    w_step(0, 0)
     for part in range(4):
         dq_step(0, 1, part)
     join_second(1)
+    w_step(1, 0)
     for part in range(4):
-        dq_step(0, 2 % hops, part) if hops > 2 else None
+        dq_step(0, 2, part)
     join_last(1)
-    tasks.extend(grad_tasks(1, 4))
+    tasks.extend(grad_tasks(1, 8))
     for step in range(3, hops):
         for part in range(4):
             dq_step(0, step, part)
-            fill()
+            fill(2)
     fill(len(tasks))
     for part in range(4):
         dq_step(1, 0, part)
+    w_step(2, 0)
     pick(1)
     share(1)
-    flip()
-    for part in range(heads):
-        w_step(0, part)
+    flip(1)
+    w_step(0, 1)
     for part in range(4):
         dq_end(0, part)
+    w_step(3, 0)
+    for part in range(4):
+        dq_step(1, 1, part)
+    w_step(1, 1)
     for number in range(2):
         for way in (0, 2):
             weight_piece(number, way).wait_recv()
@@ -651,21 +670,21 @@
         for number in range(2):
             for away in range(1, tp):
                 passage_piece(head, number, away).wait_recv()
+    load_own.wait()
     tasks.extend([functools.partial(store_slab, number) for number in range(features // slab)])
-    load_own.wait()
     ending = 64
     tasks.extend([functools.partial(store_end, first, min(ending, quarter - first)) for first in range(0, quarter, ending)])
-    for step in range(1, hops):
+    tasks.append(functools.partial(w_end, 0))
+    for step in range(2, hops):
         for part in range(4):
             dq_step(1, step, part)
             fill()
-        for part in range(heads):
-            w_step(step, part)
+        w_step(step, 1)
+        fill()
     fill(len(tasks))
     for part in range(4):
         dq_end(1, part)
-    for part in range(heads):
-        w_end(part)
+    w_end(1)
     for copy in sends:
         copy.wait_send()
 
@@ -683,10 +702,9 @@
     total = n * blocks
     hops = n // 2
     feats = features // n
-    named = jnp.pad(owners * passages + slots, ((0, 0), (0, 128 - per_block)), constant_values=-1)
     blocked = [one.reshape(blocks, block_len, width) for one in (queries, gate_pre, cotangent)]
     vmem = pl.BlockSpec(memory_space=pltpu.VMEM)
-    anywhere = pl.BlockSpec(memory_space=pl.ANY)
+    anywhere = pl.BlockSpec(memory_space=pltpu.HBM)
     half, wide = jnp.bfloat16, jnp.float32
     dma = pltpu.SemaphoreType.DMA
 
@@ -700,9 +718,14 @@
             jax.ShapeDtypeStruct((quarter, features), wide),
             jax.ShapeDtypeStruct((feats, width), wide),
         ),
-        in_specs=[anywhere] * 6 + [vmem] * 2,
+        in_specs=[anywhere] * 9,
         out_specs=(vmem,) * 3,
         scratch_shapes=[
+            pltpu.VMEM((1, features), wide),
+            pltpu.VMEM((per_block, blocks), jnp.int32),
+            pltpu.VMEM((per_block, blocks), jnp.int32),
+            pltpu.VMEM((8, 128), wide),
+            pltpu.VMEM((blocks, 128), jnp.int32),
             per_head((total, block_len, HD), half),
             per_head((total, block_len, HD), half),
             pltpu.VMEM((n, blocks, 128), jnp.int32),
@@ -720,17 +743,17 @@
             per_head((n, 2, blocks, block_len), wide),
             per_head((total + 4, 2, block_len), wide),
             per_head((total, block_len, HD), half),
-            per_head((total, PLEN, HD), half),
-            per_head((total, PLEN, HD), half),
+            pltpu.VMEM((total, PLEN, HD), half),
+            pltpu.VMEM((total, PLEN, HD), half),
             per_head((rows_dev, HD), half),
             per_head((rows_dev, HD), half),
-            pltpu.VMEM((width, rows_dev), half),
+            pltpu.VMEM((heads, HD, rows_dev), half),
             pltpu.VMEM((quarter, 2 * tp * width), half),
+            per_head((blocks, block_len, HD), half),
             per_head((2, hops, blocks, block_len, HD), half),
-            per_head((2, hops, blocks, block_len, HD), half),
-            pltpu.VMEM((2, hops, width, feats), half),
-            pltpu.VMEM((2, hops, width, feats), half),
-            dma((heads + 5,)),
+            pltpu.VMEM((heads, HD, feats), half),
+            pltpu.VMEM((2, hops, heads, HD, feats), half),
+            dma((heads + 8,)),
             dma((2,)),
             dma((heads, 2, hops, 4)),
             dma((heads, 2, hops, 4)),
@@ -749,9 +772,9 @@
             dma((1,)),
         ],
         cost_estimate=pl.CostEstimate(flops=2 * 10**10, bytes_accessed=3 * 10**7, transcendentals=0),
-        compiler_params=pltpu.CompilerParams(collective_id=0, has_side_effects=True, vmem_limit_bytes=60 << 20),
+        compiler_params=pltpu.CompilerParams(collective_id=0, has_side_effects=True, vmem_limit_bytes=VMEM_LIMIT),
         name="whole",
-    )(*blocked, store, w_key, w_value, store_gain[None], named)
+    )(*[pltpu.with_memory_space_constraint(one, pltpu.HBM) for one in (*blocked, store, w_key, w_value, store_gain[None], owners.T, slots.T)])
 
 
 def fits(queries, store, owners):

time: 162 us -> 150 us (0.926)
  Pallas kernels: 152 us -> 146 us
  local copies, waits for them, and re-layouts: 8.66 us -> 3.17 us
    pallas_call x1, Pallas kernels: 152 us -> 146 us  [query_plan(): pl.pallas_call(functools.partial(whole_kernel, n, tp), out_shape=(jax.Sha...]
    unnamed x7 -> x3, local copies, waits for them, and re-layouts: 8.06 us -> 3.17 us
where the time goes in v2:
time: 150 us
  Pallas kernels  146 us (97%)
  local copies, waits for them, and re-layouts  3.17 us (2%)
    pallas_call x1, Pallas kernels, query_plan(): pl.pallas_call(functools.partial(whole_kernel, n, tp), out_shape=(jax.Sha...  146 us
    unnamed x3, local copies, waits for them, and re-layouts  3.17 us

profile of v2, /device:TPU:0, one launch (start us, length us, event | category | flops | bytes accessed | tf_op | source)
XLA Modules:
  0.0 149.8 jit_solution(13417337037537861379)
XLA Ops:
  0.6 146.0 %whole.1 = (f32[1024,256]{1,0:T(8,128)S(1)}, f32[320,2048]{1,0:T(8,128)S(1)}, f32[256,256]{1,0:T(8,128)S(1)}) custom-call(bf16[8,128,256]{2,1,0:T(8,128)(2,1)} %bitcast.6, bf16[8,128,256]{2,1,0:T(8,128)(2,1)} %bitcast.7, bf16[8,128,256]{2,1,0:T(8,128)(2,1)} %bitcast.8, bf16[1280,2048]{1,0:T(8,128)(2,1)} %x_hbm.1, bf16[2048,256]{1,0:T(8,128)(2,1)} %wk_hbm.1, ...), custom_call_target="tpu_custom_call" | custom-call | flops 20000000000 | bytes 30000000 | tf_op jit(solution)/shard_map/whole/pallas_call | solution.py:714
  146.6 1.0 copy.15
  147.6 1.5 copy.16
  149.1 0.7 copy.17

commit v3 on v2

--- a/solution.py
+++ b/solution.py
@@ -256,14 +256,14 @@
     for copy in load_small[:2] + loads + [load_gate, load_cot] + load_w + load_small[2:] + [load_x(0), load_own]:
         copy.start()
 
-    sends = []
-
     def begin(copy):
         copy.start()
-        sends.append(copy)
 
     def remote(src, dst, send_sem, recv_sem, **to):
         return pltpu.make_async_remote_copy(src_ref=src, dst_ref=dst, send_sem=send_sem, recv_sem=recv_sem, device_id=to, device_id_type=MESH)
+
+    def whole_batch(ref, send_sem, recv_sem):
+        return remote(ref, ref, send_sem, recv_sem, st=right)
 
     parts = ((0, 0), (0, 1), (1, 0), (1, 1))
 
@@ -272,18 +272,18 @@
         ref = (q_all, g_all)[number][head]
         origin = index_at(place - step, n) if side == 0 else index_at(place + step, n)
         at = ref.at[pl.ds(origin * blocks + which * half, half)]
-        return remote(at, at, g_send.at[head, side, step, part], g_recv.at[head, side, step, part], st=right if side == 0 else left)
+        return remote(at, at, g_send.at[head, number], g_recv.at[head, side, step, part], st=right if side == 0 else left)
 
     def goes(side, step, part):
         return step < hops - 1 or parts[part][1] == side
 
     def ids_piece(away):
-        return remote(named_ref, i_all.at[me], i_send.at[away], i_recv.at[away], st=(me + away) % n)
+        return remote(named_ref, i_all.at[me], i_send.at[0], i_recv.at[0], st=(me + away) % n)
 
     def weight_piece(number, way):
         owner = mine if way < 2 else across
         at = whole.at[:, columns(owner, number)]
-        return remote(at, at, t_send.at[number, way], t_recv.at[number, way], tp=across if way == 1 else sibling)
+        return remote(at, at, t_send.at[number], t_recv.at[number, way], tp=across if way == 1 else sibling)
 
     def make_grad_in():
         load_gate.wait()
@@ -311,8 +311,7 @@
                 table[head][pl.ds(chunk * per, per)] = out[:, head * HD:(head + 1) * HD].reshape(per, PLEN, HD)
 
     def make_table():
-        for away in range(1, n):
-            ids_piece(away).wait_recv()
+        whole_batch(i_all.at[pl.ds(0, n - 1)], i_send.at[0], i_recv.at[0]).wait_recv()
         tab_buf[...] = rows_of_table(i_all[...].reshape(total, 128), me * passages, passages)
         copy = pltpu.make_async_copy(tab_buf, tab, tab_sem.at[0])
         copy.start()
@@ -340,7 +339,11 @@
         return remote(
             stats[head].at[peer] if phase == 0 else at,
             got[head].at[me] if phase == 0 else at,
-            j_send.at[head, phase, away], j_recv.at[head, phase, away], st=peer)
+            j_send.at[head, phase], j_recv.at[head, phase], st=peer)
+
+    def join_batch(head, phase):
+        ref = got[head].at[pl.ds(0, n - 1)] if phase == 0 else joined[head].at[pl.ds(0, (n - 1) * blocks)]
+        return whole_batch(ref, j_send.at[head, phase], j_recv.at[head, phase])
 
     def join_first(head):
         for away in range(1, n):
@@ -348,8 +351,7 @@
         got[head][me] = stats[head][me]
 
     def join_second(head):
-        for away in range(1, n):
-            join_piece(head, 0, away).wait_recv()
+        join_batch(head, 0).wait_recv()
         logs = [got[head][owner, 0] for owner in range(n)]
         top = functools.reduce(jnp.maximum, logs)
         shares = [jnp.exp(one - top) for one in logs]
@@ -363,8 +365,7 @@
             begin(join_piece(head, 1, away))
 
     def join_last(head):
-        for away in range(1, n):
-            join_piece(head, 1, away).wait_recv()
+        join_batch(head, 1).wait_recv()
 
     lanes = 4
 
@@ -419,7 +420,11 @@
         peer = (mine + away) % tp
         rows = pl.ds(pl.multiple_of(peer * quarter, 16), quarter)
         return remote((pk, pv)[number][head].at[rows], own_kv.at[:, own_columns(mine, head, number)],
-                      p_send.at[head, number, away], p_recv.at[head, number, away], tp=peer)
+                      p_send.at[head, number], p_recv.at[head, number], tp=peer)
+
+    def passage_batch(head, number):
+        ref = (pk, pv)[number][head].at[pl.ds(0, (tp - 1) * quarter)]
+        return remote(ref, ref, p_send.at[head, number], p_recv.at[head, number], tp=sibling)
 
     def share(head):
         for number in range(2):
@@ -438,7 +443,7 @@
         at = pl.ds(dq_parts[part][0], dq_count)
         src = dq_recv[head].at[side, step - 1, at] if step > 0 else dq_send[head].at[at]
         return remote(src, dq_recv[head].at[side, step, at],
-                      s_send.at[head, side, step, part], s_recv.at[head, side, step, part], st=right if side == 0 else left)
+                      s_send.at[head], s_recv.at[head, side, step, part], st=right if side == 0 else left)
 
     def dest_of(side, step):
         distance = hops - step
@@ -473,10 +478,13 @@
                 value = value + dq_recv[head][side, hops - 1, block].astype(jnp.float32)
             dq_ref[pl.ds(block * block_len, block_len), pl.ds(head * HD, HD)] = value
 
+    def w_at(side, step, part):
+        return (side * hops + step) * heads + part
+
     def w_piece(side, step, part):
-        src = w_recv.at[side, step - 1, part] if step > 0 else w_send.at[part]
-        return remote(src, w_recv.at[side, step, part],
-                      ws_send.at[side, step, part], ws_recv.at[side, step, part], st=right if side == 0 else left)
+        src = w_recv.at[w_at(side, step - 1, part)] if step > 0 else w_send.at[part]
+        return remote(src, w_recv.at[w_at(side, step, part)],
+                      ws_send.at[0], ws_recv.at[side, step, part], st=right if side == 0 else left)
 
     def w_term(dest, part):
         return dot(pv_flip[part], normed[:, pl.ds(pl.multiple_of(dest * feats, 128), feats)])
@@ -491,9 +499,9 @@
             value = w_term(dest_of(side, step), part)
             if step > 0 and w_used(side, step - 1, part):
                 w_piece(side, step - 1, part).wait_recv()
-                value = value + w_recv[side, step - 1, part].astype(jnp.float32)
+                value = value + w_recv[w_at(side, step - 1, part)].astype(jnp.float32)
             if step > 0:
-                w_recv[side, step - 1, part] = value.astype(jnp.bfloat16)
+                w_recv[w_at(side, step - 1, part)] = value.astype(jnp.bfloat16)
             else:
                 w_send[part] = value.astype(jnp.bfloat16)
             begin(w_piece(side, step, part))
@@ -502,7 +510,7 @@
         value = w_term(me, part)
         for side in range(2):
             w_piece(side, hops - 1, part).wait_recv()
-            value = value + w_recv[side, hops - 1, part].astype(jnp.float32)
+            value = value + w_recv[w_at(side, hops - 1, part)].astype(jnp.float32)
         gw_ref[:, pl.ds(part * HD, HD)] = value.T
 
     def flip(head):
@@ -636,19 +644,25 @@
     gather_rest(1, False)
     make_stats(1, index_at(place + hops, n))
     join_first(1)
-    w_step(0, 0)
-    for part in range(4):
+    for part in range(2):
         dq_step(0, 1, part)
     join_second(1)
-    w_step(1, 0)
-    for part in range(4):
+    for part in range(2, 4):
+        dq_step(0, 1, part)
+    w_step(0, 0)
+    for part in range(2):
         dq_step(0, 2, part)
     join_last(1)
     tasks.extend(grad_tasks(1, 8))
+    for part in range(2, 4):
+        dq_step(0, 2, part)
+        fill()
+    w_step(1, 0)
+    fill()
     for step in range(3, hops):
         for part in range(4):
             dq_step(0, step, part)
-            fill(2)
+            fill()
     fill(len(tasks))
     for part in range(4):
         dq_step(1, 0, part)
@@ -659,17 +673,16 @@
     w_step(0, 1)
     for part in range(4):
         dq_end(0, part)
-    w_step(3, 0)
     for part in range(4):
         dq_step(1, 1, part)
+    w_step(3, 0)
     w_step(1, 1)
     for number in range(2):
         for way in (0, 2):
             weight_piece(number, way).wait_recv()
     for head in range(heads):
         for number in range(2):
-            for away in range(1, tp):
-                passage_piece(head, number, away).wait_recv()
+            passage_batch(head, number).wait_recv()
     load_own.wait()
     tasks.extend([functools.partial(store_slab, number) for number in range(features // slab)])
     ending = 64
@@ -685,8 +698,18 @@
     for part in range(4):
         dq_end(1, part)
     w_end(1)
-    for copy in sends:
-        copy.wait_send()
+    for head in range(heads):
+        for number in range(2):
+            ref = (q_all, g_all)[number][head].at[pl.ds(0, (n - 1) * blocks)]
+            whole_batch(ref, g_send.at[head, number], g_recv.at[head, 0, 0, 0]).wait_send()
+            join_batch(head, number).wait_send()
+            passage_batch(head, number).wait_send()
+        whole_batch(dq_sorted[head].at[pl.ds(0, (n - 1) * blocks)], s_send.at[head], s_recv.at[head, 0, 0, 0]).wait_send()
+    for number in range(2):
+        ref = whole.at[:, pl.ds(0, (tp - 1) * width)]
+        remote(ref, ref, t_send.at[number], t_recv.at[number, 0], tp=sibling).wait_send()
+    whole_batch(w_recv.at[pl.ds(0, (n - 1) * heads)], ws_send.at[0], ws_recv.at[0, 0, 0]).wait_send()
+    whole_batch(i_all.at[pl.ds(0, n - 1)], i_send.at[0], i_recv.at[0]).wait_send()
 
 
 def query_plan(queries, gate_pre, cotangent, store, store_gain, w_key, w_value, owners, slots):
@@ -752,22 +775,22 @@
             per_head((blocks, block_len, HD), half),
             per_head((2, hops, blocks, block_len, HD), half),
             pltpu.VMEM((heads, HD, feats), half),
-            pltpu.VMEM((2, hops, heads, HD, feats), half),
+            pltpu.VMEM((2 * hops * heads, HD, feats), half),
             dma((heads + 8,)),
             dma((2,)),
+            dma((heads, 2)),
             dma((heads, 2, hops, 4)),
+            dma((1,)),
+            dma((1,)),
+            dma((heads, 2)),
+            dma((heads, 2)),
+            dma((heads,)),
             dma((heads, 2, hops, 4)),
-            dma((n,)),
-            dma((n,)),
-            dma((heads, 2, n)),
-            dma((heads, 2, n)),
-            dma((heads, 2, hops, 4)),
-            dma((heads, 2, hops, 4)),
+            dma((1,)),
             dma((2, hops, heads)),
-            dma((2, hops, heads)),
-            dma((heads, 2, tp)),
-            dma((heads, 2, tp)),
-            dma((2, 3)),
+            dma((heads, 2)),
+            dma((heads, 2)),
+            dma((2,)),
             dma((2, 3)),
             dma((1,)),
         ],

time: 150 us -> 146 us (0.973)
  Pallas kernels: 146 us -> 142 us
    pallas_call x1, Pallas kernels: 146 us -> 142 us  [query_plan(): pl.pallas_call(functools.partial(whole_kernel, n, tp), out_shape=(jax.Sha...]
where the time goes in v3:
time: 146 us
  Pallas kernels  142 us (97%)
  local copies, waits for them, and re-layouts  3.17 us (2%)
    pallas_call x1, Pallas kernels, query_plan(): pl.pallas_call(functools.partial(whole_kernel, n, tp), out_shape=(jax.Sha...  142 us
    unnamed x3, local copies, waits for them, and re-layouts  3.17 us

profile of v3, /device:TPU:0, one launch (start us, length us, event | category | flops | bytes accessed | tf_op | source)
XLA Modules:
  0.0 145.7 jit_solution(141797400727480670)
XLA Ops:
  0.6 141.9 %whole.1 = (f32[1024,256]{1,0:T(8,128)S(1)}, f32[320,2048]{1,0:T(8,128)S(1)}, f32[256,256]{1,0:T(8,128)S(1)}) custom-call(bf16[8,128,256]{2,1,0:T(8,128)(2,1)} %bitcast.6, bf16[8,128,256]{2,1,0:T(8,128)(2,1)} %bitcast.7, bf16[8,128,256]{2,1,0:T(8,128)(2,1)} %bitcast.8, bf16[1280,2048]{1,0:T(8,128)(2,1)} %x_hbm.1, bf16[2048,256]{1,0:T(8,128)(2,1)} %wk_hbm.1, ...), custom_call_target="tpu_custom_call" | custom-call | flops 20000000000 | bytes 30000000 | tf_op jit(solution)/shard_map/whole/pallas_call | solution.py:737
  142.5 1.0 copy.15
  143.5 1.5 %copy.16 = f32[320,2048]{1,0:T(8,128)} copy(f32[320,2048]{1,0:T(8,128)S(1)} %get-tuple-element.7) | data formatting | bytes 5242880
  145.0 0.7 copy.17

commit v4 on v3

--- a/solution.py
+++ b/solution.py
@@ -531,13 +531,6 @@
         value = gs_ref[rows]
         gs_ref[rows] = inverse * (value - unit * jnp.mean(value * unit, axis=-1, keepdims=True))
 
-    for copy in load_small[:2]:
-        copy.wait()
-    per_block = owners_buf.shape[0]
-    flat[...] = jnp.full(flat.shape, -1.0, jnp.float32)
-    flat[pl.ds(0, per_block), pl.ds(0, blocks)] = (owners_buf[...] * passages + slots_buf[...]).astype(jnp.float32)
-    named_ref[...] = jnp.full(named_ref.shape, -1, jnp.int32)
-    named_ref[:, pl.ds(0, 8)] = flat[...].T[:blocks].astype(jnp.int32)
     loads[0].wait()
     pl.semaphore_wait(barrier, n - 1 + tp - 1)
     for part in range(2):
@@ -547,6 +540,13 @@
     for part in range(2, 4):
         for side in range(2):
             begin(gather_piece(0, side, 0, part))
+    for copy in load_small[:2]:
+        copy.wait()
+    per_block = owners_buf.shape[0]
+    flat[...] = jnp.full(flat.shape, -1.0, jnp.float32)
+    flat[pl.ds(0, per_block), pl.ds(0, blocks)] = (owners_buf[...] * passages + slots_buf[...]).astype(jnp.float32)
+    named_ref[...] = jnp.full(named_ref.shape, -1, jnp.int32)
+    named_ref[:, pl.ds(0, 8)] = flat[...].T[:blocks].astype(jnp.int32)
     for away in range(1, n):
         begin(ids_piece(away))
     i_all[me] = named_ref[...]
@@ -712,6 +712,17 @@
     whole_batch(i_all.at[pl.ds(0, n - 1)], i_send.at[0], i_recv.at[0]).wait_send()
 
 
+def put_kernel(dq_ref, gs_ref, gw_ref, dq_out, gs_out, gw_out, sem):
+    copies = [
+        pltpu.make_async_copy(src, dst, sem.at[number])
+        for number, (src, dst) in enumerate(((gs_ref, gs_out), (dq_ref, dq_out), (gw_ref, gw_out)))
+    ]
+    for copy in copies:
+        copy.start()
+    for copy in copies:
+        copy.wait()
+
+
 def query_plan(queries, gate_pre, cotangent, store, store_gain, w_key, w_value, owners, slots):
     n = lax.axis_size("st")
     tp = lax.axis_size("tp")
@@ -734,7 +745,7 @@
     def per_head(shape, kind):
         return [pltpu.VMEM(shape, kind) for _ in range(heads)]
 
-    return pl.pallas_call(
+    results = pl.pallas_call(
         functools.partial(whole_kernel, n, tp),
         out_shape=(
             jax.ShapeDtypeStruct((tok_rows, width), wide),
@@ -798,6 +809,16 @@
         compiler_params=pltpu.CompilerParams(collective_id=0, has_side_effects=True, vmem_limit_bytes=VMEM_LIMIT),
         name="whole",
     )(*[pltpu.with_memory_space_constraint(one, pltpu.HBM) for one in (*blocked, store, w_key, w_value, store_gain[None], owners.T, slots.T)])
+    return pl.pallas_call(
+        put_kernel,
+        out_shape=tuple(jax.ShapeDtypeStruct(one.shape, one.dtype) for one in results),
+        in_specs=[vmem] * 3,
+        out_specs=(anywhere,) * 3,
+        scratch_shapes=[dma((3,))],
+        cost_estimate=pl.CostEstimate(flops=10**7, bytes_accessed=8 * 10**6, transcendentals=0),
+        compiler_params=pltpu.CompilerParams(vmem_limit_bytes=8 << 20),
+        name="put",
+    )(*results)
 
 
 def fits(queries, store, owners):

time: 146 us -> 145 us (level)
  local copies, waits for them, and re-layouts: 3.17 us -> 0 us
  Pallas kernels: 142 us -> 144 us
    unnamed x3 -> x0, local copies, waits for them, and re-layouts: 3.17 us -> none
    pallas_call x0 -> x1, Pallas kernels: none -> 1.94 us  [query_plan(): pl.pallas_call(put_kernel, out_shape=tuple((jax.ShapeDtypeStruct(one.shap...]
where the time goes in v4:
time: 145 us
  Pallas kernels  144 us (99%)
    pallas_call x1, Pallas kernels, query_plan(): pl.pallas_call(functools.partial(whole_kernel, n, tp), out_shape=(jax.Sha...  142 us

profile of v4, /device:TPU:0, one launch (start us, length us, event | category | flops | bytes accessed | tf_op | source)
XLA Modules:
  0.0 144.6 jit_solution(17440987059192973902)
XLA Ops:
  0.6 141.9 %whole.1 = (f32[1024,256]{1,0:T(8,128)S(1)}, f32[320,2048]{1,0:T(8,128)S(1)}, f32[256,256]{1,0:T(8,128)S(1)}) custom-call(bf16[8,128,256]{2,1,0:T(8,128)(2,1)} %bitcast.6, bf16[8,128,256]{2,1,0:T(8,128)(2,1)} %bitcast.7, bf16[8,128,256]{2,1,0:T(8,128)(2,1)} %bitcast.8, bf16[1280,2048]{1,0:T(8,128)(2,1)} %x_hbm.1, bf16[2048,256]{1,0:T(8,128)(2,1)} %wk_hbm.1, ...), custom_call_target="tpu_custom_call" | custom-call | flops 20000000000 | bytes 30000000 | tf_op jit(solution)/shard_map/whole/pallas_call | solution.py:748
  142.5 1.9 %put.1 = (f32[1024,256]{1,0:T(8,128)}, f32[320,2048]{1,0:T(8,128)}, f32[256,256]{1,0:T(8,128)}) custom-call(f32[1024,256]{1,0:T(8,128)S(1)} %get-tuple-element.6.dq_ref, f32[320,2048]{1,0:T(8,128)S(1)} %get-tuple-element.7.gs_ref, f32[256,256]{1,0:T(8,128)S(1)} %get-tuple-element.8.gw_ref), custom_call_target="tpu_custom_call" | custom-call | flops 10000000 | bytes 8000000 | tf_op jit(solution)/shard_map/put/pallas_call | solution.py:812

commit v5 on v4

--- a/solution.py
+++ b/solution.py
@@ -588,14 +588,14 @@
         edges = [turns * piece // pieces for piece in range(pieces + 1)]
         return [grads_task(head, edges[piece], edges[piece + 1]) for piece in range(pieces)]
 
-    def gather_step(head, step):
+    def gather_step(head, step, count=1):
         for part in range(4):
             for side in range(2):
                 if goes(side, step, part):
                     if step > 0:
                         gather_piece(head, side, step - 1, part).wait_recv()
                     begin(gather_piece(head, side, step, part))
-            fill()
+            fill(count)
 
     def gather_rest(head, first):
         if first:
@@ -630,13 +630,15 @@
     gather_step(1, 1)
     tasks.extend([both(1, 1), idle, idle, functools.partial(join_last, 0)])
     gather_step(1, 2)
-    tasks.extend(grad_tasks(0, 4))
-    tasks.extend([functools.partial(pick, 0), functools.partial(share, 0), functools.partial(flip, 0)])
+    tasks.extend(grad_tasks(0, 6))
     for step in range(3, hops):
-        gather_step(1, step)
+        gather_step(1, step, 2)
     fill(len(tasks))
     for part in range(4):
         dq_step(0, 0, part)
+    pick(0)
+    share(0)
+    flip(0)
     for step in range(2, hops - 1):
         both(1, step)()
     gather_rest(1, True)

time: 145 us -> 145 us (level)
  no operation moved by 1% of the time
where the time goes in v5:
time: 145 us
  Pallas kernels  144 us (99%)
    pallas_call x1, Pallas kernels, query_plan(): pl.pallas_call(functools.partial(whole_kernel, n, tp), out_shape=(jax.Sha...  142 us

profile of v5, /device:TPU:0, one launch (start us, length us, event | category | flops | bytes accessed | tf_op | source)
XLA Modules:
  0.0 144.7 jit_solution(7940562259874247291)
XLA Ops:
  0.6 141.9 %whole.1 = (f32[1024,256]{1,0:T(8,128)S(1)}, f32[320,2048]{1,0:T(8,128)S(1)}, f32[256,256]{1,0:T(8,128)S(1)}) custom-call(bf16[8,128,256]{2,1,0:T(8,128)(2,1)} %bitcast.6, bf16[8,128,256]{2,1,0:T(8,128)(2,1)} %bitcast.7, bf16[8,128,256]{2,1,0:T(8,128)(2,1)} %bitcast.8, bf16[1280,2048]{1,0:T(8,128)(2,1)} %x_hbm.1, bf16[2048,256]{1,0:T(8,128)(2,1)} %wk_hbm.1, ...), custom_call_target="tpu_custom_call" | custom-call | flops 20000000000 | bytes 30000000 | tf_op jit(solution)/shard_map/whole/pallas_call | solution.py:750
  142.5 1.9 %put.1 = (f32[1024,256]{1,0:T(8,128)}, f32[320,2048]{1,0:T(8,128)}, f32[256,256]{1,0:T(8,128)}) custom-call(f32[1024,256]{1,0:T(8,128)S(1)} %get-tuple-element.6.dq_ref, f32[320,2048]{1,0:T(8,128)S(1)} %get-tuple-element.7.gs_ref, f32[256,256]{1,0:T(8,128)S(1)} %get-tuple-element.8.gw_ref), custom_call_target="tpu_custom_call" | custom-call | flops 10000000 | bytes 8000000 | tf_op jit(solution)/shard_map/put/pallas_call | solution.py:814
